TPU v7x, 512 devices: a whole 4x4x16 slice. The times are simulated.
512 devices in a mesh: sp: 64 (over z, y), tp: 8 (over x, core).
Axes of the slice: x: 4, y: 4, z: 16, core: 2. Of those that a mesh axis runs over, the one named last changes fastest.
Arguments:
- stream_in: bfloat16 [16384, 2048], P('sp'), may hold values from -6 to 6
- norm_gain: float32 [2, 2048], replicated, may hold values from 0.1 to 1.9
- value_weight: bfloat16 [2, 2048, 2048], P(None, 'sp', 'tp'), may hold values from -0.125 to 0.125
- gate_weight: bfloat16 [2, 2048, 2048], P(None, 'sp', 'tp'), may hold values from -0.125 to 0.125
- conv_taps: float32 [2, 31, 2048], P(None, None, 'tp'), may hold values from -5 to 5
- channel_gain: float32 [2, 2048], P(None, 'tp'), may hold values from 0.1 to 1.9
- out_weight: bfloat16 [2, 2048, 2048], P(None, 'tp', 'sp'), may hold values from -0.125 to 0.125
Outputs:
- stream_out: bfloat16 [16384, 2048], P('sp')
All inputs are finite; a program needn't handle non-finite values.
Results may differ from a plain program's by a relative error of at most 0.015.
Values may be sent and summed in bfloat16 or wider, within the bound.
A program may use at most 64 MiB of HBM per device.

v0:
```python
import jax
import jax.numpy as jnp
from jax import lax
from jax.sharding import Mesh
from jax.sharding import PartitionSpec as P

LAYERS = 2
SP = ("sp_0", "sp_1")


epsilon = 1e-05


def side_by_side(arrays, axis, dim, along):
    widths = [a.shape[along] for a in arrays]
    both = jnp.concatenate(arrays, axis=along)
    out = lax.all_gather(both, axis, axis=dim, tiled=True)
    return tuple(jnp.split(out, [sum(widths[:k]) for k in range(1, len(widths))], axis=along))


def passed_along(value, axis, steps):
    count = lax.axis_size(axis)
    leading, last = (max(0, -steps), min(count, count - steps))
    return lax.ppermute(value, axis, [(source, source + steps) for source in range(leading, last)])


def sent_to_all(shard, axis):
    copies = jnp.broadcast_to(shard, (lax.axis_size(axis), *shard.shape))
    return lax.all_to_all(copies, axis, split_axis=0, concat_axis=0, tiled=True)


def over_copies(shard, axis):
    return sent_to_all(shard, axis).sum(axis=0)


def together(arrays, axis):
    ends = [0]
    for a in arrays:
        ends.append(ends[-1] + a.size)
    total = over_copies(jnp.concatenate([a.ravel() for a in arrays]), axis)
    return tuple((total[b:e].reshape(a.shape) for a, b, e in zip(arrays, ends, ends[1:])))


def gathered_by_axis(shard, axes, dim):
    if not axes:
        return shard
    nearer = lax.all_gather(shard, axes[-1], axis=dim, tiled=True)
    return gathered_by_axis(nearer, axes[:-1], dim)


def in_blocks(shard, dim, peers):
    before, after = (shard.shape[:dim], shard.shape[dim + 1 :])
    return jnp.moveaxis(shard.reshape(*before, peers, -1, *after), dim, 0)


def summed_on_arrival(shard, axis, dim):
    peers = lax.axis_size(axis)
    parts = lax.all_to_all(in_blocks(shard, dim, peers), axis, 0, 0, tiled=True)
    return jnp.sum(parts.astype(jnp.float32), axis=0)


def laid_out(parts, dim):
    parts = jnp.moveaxis(parts, 0, dim)
    lengths = parts.shape
    return parts.reshape(*lengths[:dim], lengths[dim] * lengths[dim + 1], *lengths[dim + 2 :])


def gather_directly(shard, axis, dim):
    return laid_out(sent_to_all(shard, axis), dim)


def body(stream_in, norm_gain, value_weight, gate_weight, conv_taps, channel_gain, out_weight):
    stream = stream_in
    tok_rows = stream_in.shape[0]
    width = stream_in.shape[1]
    kernel = conv_taps.shape[1]
    local_cols = value_weight.shape[2]
    for layer in range(LAYERS):
        wide = stream.astype(jnp.float32)
        normed = (
            wide
            * lax.rsqrt(jnp.mean(wide * wide, axis=1, keepdims=True) + epsilon)
            * norm_gain[layer]
        ).astype(jnp.bfloat16)
        full_value, full_gate = side_by_side((value_weight[layer], gate_weight[layer]), SP, 0, 1)
        value = jnp.dot(normed, full_value, preferred_element_type=jnp.float32)
        gate = jnp.dot(normed, full_gate, preferred_element_type=jnp.float32)
        gated = (value * jax.nn.sigmoid(gate)).astype(jnp.bfloat16)
        earlier = passed_along(gated[tok_rows - (kernel - 1) :], SP, 1)
        padded = jnp.concatenate([earlier, gated], axis=0).astype(jnp.float32)
        taps = conv_taps[layer]
        filtered = jnp.zeros((tok_rows, local_cols), jnp.float32)
        for tap in range(kernel):
            filtered = filtered + taps[tap] * padded[tap : tap + tok_rows]
        sum_first, sum_second = together(
            (jnp.sum(filtered, axis=1), jnp.sum(filtered * filtered, axis=1)), "tp"
        )
        mean_value = (sum_first / width)[:, None]
        variance = (sum_second / width)[:, None] - mean_value * mean_value
        activated = jax.nn.silu(
            (filtered - mean_value) * lax.rsqrt(variance + epsilon) * channel_gain[layer]
        ).astype(jnp.bfloat16)
        full_out = gathered_by_axis(out_weight[layer], SP, 1)
        share = tok_rows // lax.axis_size("tp")
        summed_rows = summed_on_arrival(
            jnp.dot(activated, full_out, preferred_element_type=jnp.float32).astype(jnp.bfloat16),
            "tp",
            0,
        )
        own_rows = lax.dynamic_slice_in_dim(wide, lax.axis_index("tp") * share, share, 0)
        stream = gather_directly((own_rows + summed_rows).astype(jnp.bfloat16), "tp", 0)
    return stream


def solution(mesh):
    finer = Mesh(mesh.devices.reshape(16, 4, mesh.shape["tp"]), ("sp_0", "sp_1", "tp"))
    placed = (
        P(SP, None),
        P(),
        P(None, SP, "tp"),
        P(None, SP, "tp"),
        P(None, None, "tp"),
        P(None, "tp"),
        P(None, "tp", SP),
    )
    return jax.shard_map(body, mesh=finer, in_specs=placed, out_specs=P(SP, None), check_vma=False)
```

profile of v0, /device:TPU:1, one launch (start us, length us, event | category | flops | bytes accessed | tf_op | source)
XLA Modules:
  0.0 482.7 jit_solution(8478346066151861120)
XLA Ops:
  8.7 11.0 %all-gather = bf16[1,256,128]{1,2,0:T(8,128)(2,1)} all-gather(bf16[1,256,32]{1,2,0:T(8,128)(2,1)S(1)} %get-tuple-element.79), channel_id=2, replica_groups=mesh['sp_0'=16,'sp_1'=4,'tp'=8] {'sp_1'}, dimensions={2}, use_global_device_ids=true | all-gather | bytes 81920 | tf_op jit(solution)/shard_map/all_gather | solution.py:47
  23.1 1.5 multiply_reduce_fusion.1
  24.7 122.1 %all-gather.9.cloned.1.call-done = bf16[2048,512]{1,0:T(8,128)(2,1)} async-done(((bf16[32,512]{1,0:T(8,128)(2,1)}), bf16[2048,512]{1,0:T(8,128)(2,1)}) %all-gather.9.cloned.1.call-update) | async-done | bytes 2097168 | tf_op jit(solution)/shard_map/all_gather | solution.py:17
  146.8 2.2 fusion.14
  149.5 2.2 collective-permute-start
  154.5 15.4 %all-to-all-start = ((f32[8,1,512]{2,1,0:T(1,128)}), f32[8,1,512]{2,1,0:T(1,128)S(1)}, u32[]{:S(2)}, u32[]{:S(2)}) async-start(f32[8,1,512]{2,1,0:T(1,128)} %broadcast_in_dim.8), calls=%async_computation | async-start | bytes 32768 | tf_op jit(solution)/shard_map/all_to_all | solution.py:29
  169.8 4.6 all-to-all-done
  174.5 40.2 %all-gather.13.cloned.1.call-done = bf16[1,256,2048]{1,2,0:T(8,128)(2,1)} async-done(((bf16[1,256,128]{1,2,0:T(8,128)(2,1)}), bf16[1,256,2048]{1,2,0:T(8,128)(2,1)}) %all-gather.13.cloned.1.call-update) | async-done | bytes 1048592 | tf_op jit(solution)/shard_map/all_gather | solution.py:47
  214.7 2.7 convolution_convert_fusion.1
  217.4 15.6 %all-to-all-start.1 = ((bf16[8,32,2048]{2,1,0:T(8,128)(2,1)}), bf16[8,32,2048]{2,1,0:T(8,128)(2,1)S(1)}, u32[]{:S(2)}, u32[]{:S(2)}) async-start(bf16[8,32,2048]{2,1,0:T(8,128)(2,1)} %bitcast.36), calls=%async_computation.1 | async-start | bytes 2097152 | tf_op jit(solution)/shard_map/all_to_all | solution.py:58
  233.0 1.5 convert_element_type.54
  234.6 13.4 %all-to-all-done.1 = bf16[8,32,2048]{2,1,0:T(8,128)(2,1)S(1)} async-done(((bf16[8,32,2048]{2,1,0:T(8,128)(2,1)}), bf16[8,32,2048]{2,1,0:T(8,128)(2,1)S(1)}, u32[]{:S(2)}, u32[]{:S(2)}) %all-to-all-start.1) | async-done | bytes 1048608 | tf_op jit(solution)/shard_map/all_to_all | solution.py:58
  250.2 4.4 all-to-all-start.2
  254.7 10.6 %all-gather.2 = bf16[1,256,128]{1,2,0:T(8,128)(2,1)} all-gather(bf16[1,256,32]{1,2,0:T(8,128)(2,1)S(1)} %get-tuple-element.80), channel_id=4, replica_groups=mesh['sp_0'=16,'sp_1'=4,'tp'=8] {'sp_1'}, dimensions={2}, use_global_device_ids=true | all-gather | bytes 81920 | tf_op jit(solution)/shard_map/all_gather | solution.py:47
  265.3 4.4 all-to-all-done.2
  271.3 85.2 %all-gather.11.cloned.1.call-done = bf16[2048,512]{1,0:T(8,128)(2,1)} async-done(((bf16[32,512]{1,0:T(8,128)(2,1)}), bf16[2048,512]{1,0:T(8,128)(2,1)}) %all-gather.11.cloned.1.call-update) | async-done | bytes 2097168 | tf_op jit(solution)/shard_map/all_gather | solution.py:17
  356.6 2.0 fusion.11
  358.6 1.7 fusion.9
  360.3 2.2 collective-permute-start.1
  364.6 19.8 %all_to_all.32 = f32[8,1,512]{2,1,0:T(1,128)S(1)} all-to-all(f32[8,1,512]{2,1,0:T(1,128)S(1)} %broadcast_in_dim.20), channel_id=1, replica_groups=mesh['sp_0'=16,'sp_1'=4,'tp'=8] {'tp'}, dimensions={0} | all-to-all | bytes 32768 | tf_op jit(solution)/shard_map/all_to_all | solution.py:29
  384.4 40.0 %all-gather.15.cloned.1.call-done = bf16[1,256,2048]{1,2,0:T(8,128)(2,1)} async-done(((bf16[1,256,128]{1,2,0:T(8,128)(2,1)}), bf16[1,256,2048]{1,2,0:T(8,128)(2,1)}) %all-gather.15.cloned.1.call-update) | async-done | bytes 1048592 | tf_op jit(solution)/shard_map/all_gather | solution.py:47
  424.4 1.7 convolution_convert_fusion
  426.1 30.3 %all_to_all.33 = bf16[8,32,2048]{2,1,0:T(8,128)(2,1)S(1)} all-to-all(bf16[8,32,2048]{2,1,0:T(8,128)(2,1)S(1)} %bitcast.89), channel_id=1, replica_groups=mesh['sp_0'=16,'sp_1'=4,'tp'=8] {'tp'}, dimensions={0} | all-to-all | bytes 2097152 | tf_op jit(solution)/shard_map/all_to_all | solution.py:58
  456.8 18.4 %all_to_all.34 = bf16[8,32,2048]{2,1,0:T(8,128)(2,1)S(1)} all-to-all(bf16[8,32,2048]{2,1,0:T(8,128)(2,1)S(1)} %broadcast_in_dim.21), channel_id=1, replica_groups=mesh['sp_0'=16,'sp_1'=4,'tp'=8] {'tp'}, dimensions={0} | all-to-all | bytes 2097152 | tf_op jit(solution)/shard_map/all_to_all | solution.py:29
  (55 shorter events, 16.1 us)
Async XLA Ops:
  6.5 140.2 %all-gather.9.cloned.1.call-start = ((), (), s32[]{:S(2)}) async-start(), calls=%async_computation.6 | async-start | bytes 2129920 | tf_op jit(solution)/shard_map/all_gather | solution.py:17
  8.0 206.8 %all-gather.13.cloned.1.call-start = ((), (), s32[]{:S(2)}) async-start(), calls=%async_computation.8 | async-start | bytes 1114112 | tf_op jit(solution)/shard_map/all_gather | solution.py:47
  19.8 336.8 %all-gather.11.cloned.1.call-start = ((), (), s32[]{:S(2)}) async-start(), calls=%async_computation.7 | async-start | bytes 2129920 | tf_op jit(solution)/shard_map/all_gather | solution.py:17
  24.6 124.3 %copy-start = (bf16[256,2048]{1,0:T(8,128)(2,1)S(1)}, bf16[256,2048]{1,0:T(8,128)(2,1)}, u32[]{:S(2)}) copy-start(bf16[256,2048]{1,0:T(8,128)(2,1)} %param.7) | copy-start | bytes 3145732
  146.8 2.2 copy-start.3
  149.5 3.1 collective-permute-start
  152.7 17.2 %copy-start.2 = (f32[2,256]{1,0:T(2,128)S(1)}, f32[2,256]{1,0:T(2,128)}, u32[]{:S(2)}) copy-start(f32[2,256]{1,0:T(2,128)} %param.12) | copy-start | bytes 6148
  154.5 20.0 %all-to-all-start = ((f32[8,1,512]{2,1,0:T(1,128)}), f32[8,1,512]{2,1,0:T(1,128)S(1)}, u32[]{:S(2)}, u32[]{:S(2)}) async-start(f32[8,1,512]{2,1,0:T(1,128)} %broadcast_in_dim.8), calls=%async_computation | async-start | bytes 32768 | tf_op jit(solution)/shard_map/all_to_all | solution.py:29
  217.4 30.6 %all-to-all-start.1 = ((bf16[8,32,2048]{2,1,0:T(8,128)(2,1)}), bf16[8,32,2048]{2,1,0:T(8,128)(2,1)S(1)}, u32[]{:S(2)}, u32[]{:S(2)}) async-start(bf16[8,32,2048]{2,1,0:T(8,128)(2,1)} %bitcast.36), calls=%async_computation.1 | async-start | bytes 2097152 | tf_op jit(solution)/shard_map/all_to_all | solution.py:58
  250.2 19.4 %all-to-all-start.2 = ((bf16[8,32,2048]{2,1,0:T(8,128)(2,1)}), bf16[8,32,2048]{2,1,0:T(8,128)(2,1)S(1)}, u32[]{:S(2)}, u32[]{:S(2)}) async-start(bf16[8,32,2048]{2,1,0:T(8,128)(2,1)} %broadcast_in_dim.9), calls=%async_computation.2 | async-start | bytes 2097152 | tf_op jit(solution)/shard_map/all_to_all | solution.py:29
  254.7 169.7 %all-gather.15.cloned.1.call-start = ((), (), s32[]{:S(2)}) async-start(), calls=%async_computation.9 | async-start | bytes 1114112 | tf_op jit(solution)/shard_map/all_gather | solution.py:47
  271.3 87.2 %copy-start.1 = (bf16[256,2048]{1,0:T(8,128)(2,1)S(1)}, bf16[256,2048]{1,0:T(8,128)(2,1)}, u32[]{:S(2)}) copy-start(bf16[256,2048]{1,0:T(8,128)(2,1)} %get-tuple-element.10) | copy-start | bytes 3145732
  360.3 3.1 collective-permute-start.1
Sparse Core Ops, SparseCore 0:
  10.3 136.4 all-gather.8
  148.8 65.8 all-gather.12
  217.7 138.8 all-gather.10
  358.5 65.8 all-gather.14
where the time goes:
time: 484 us; the launch traced here: 483 us
  waiting for transfers between devices  310 us (64%)
  blocking collectives  90.1 us (19%)
  starting transfers between devices  40 us (8%)
  between operations  13.3 us (3%)
  matrix products  10.8 us (2%)
  other arithmetic  9.64 us (2%)
  local copies, waits for them, and re-layouts  8.66 us (2%)
    all_gather x2, waiting for transfers between devices, side_by_side(): out = lax.all_gather(both, axis, axis=dim, tiled=True)  207 us
    all_gather x2, waiting for transfers between devices, gathered_by_axis(): nearer = lax.all_gather(shard, axes[-1], axis=dim, tiled=True)  80.2 us
    all_to_all x2, blocking collectives, sent_to_all(): return lax.all_to_all(copies, axis, split_axis=0, concat_axis=0, tiled=True)  38.2 us
    all_to_all x1, blocking collectives, summed_on_arrival(): parts = lax.all_to_all(in_blocks(shard, dim, peers), axis, 0, 0, tiled=True)  30.3 us
    all_gather x2, blocking collectives, gathered_by_axis(): nearer = lax.all_gather(shard, axes[-1], axis=dim, tiled=True)  21.6 us
    all_to_all x2, starting transfers between devices, sent_to_all(): return lax.all_to_all(copies, axis, split_axis=0, concat_axis=0, tiled=True)  19.8 us
    all_to_all x1, starting transfers between devices, summed_on_arrival(): parts = lax.all_to_all(in_blocks(shard, dim, peers), axis, 0, 0, tiled=True)  15.6 us
    all_to_all x1, waiting for transfers between devices, summed_on_arrival(): parts = lax.all_to_all(in_blocks(shard, dim, peers), axis, 0, 0, tiled=True)  13.4 us
  transfers between devices with their start and end apart: 9, of which 8 were waited for; matrix products, arithmetic and copies ran while one was open for 5% of the time, Pallas kernels for 0%

commit v1 on v0

v1 whole, which is shorter than its diff:
```python
import jax
import jax.numpy as jnp
from jax import lax
from jax.experimental import pallas as pl
from jax.experimental.pallas import tpu as pltpu
from jax.sharding import Mesh
from jax.sharding import PartitionSpec as P

Z, Y, X, C = 16, 4, 4, 2
TP = X * C
MESH = pl.DeviceIdType.MESH
EPS = 1e-05
F32 = jnp.float32
BF16 = jnp.bfloat16
N_SEMS = 560


def sigmoid(v):
    return 0.5 + 0.5 * jnp.tanh(0.5 * v)


def kernel(
    stream_hbm, ngain, vw, gw, taps, cgain, ow, out_ref,
    vg0, vg1, ou0, ou1, xs, s1, s2, f0, f1, nb, gx, h0, h1, gb0, gb1, cg, sems,
):
    z, y, x, c = (lax.axis_index(a) for a in ("z", "y", "x", "c"))
    tp = x * C + c
    sp = z * Y + y

    used = [0]
    sent = []

    def new_sem():
        used[0] += 1
        return sems.at[used[0] - 1]

    def remote(src, dst, device, keep=True):
        copy = pltpu.make_async_remote_copy(
            src_ref=src, dst_ref=dst, send_sem=new_sem(), recv_sem=new_sem(),
            device_id=device, device_id_type=MESH,
        )
        if keep:
            sent.append(copy)
        return copy

    def local(src, dst):
        copy = pltpu.make_async_copy(src, dst, new_sem())
        copy.start()
        return copy

    def zp(d):
        return lax.rem(z + d + Z, Z)

    def yp(d):
        return lax.rem(y + d + Y, Y)

    def xp(d):
        return lax.rem(x + d + X, X)

    own_vg0 = [local(vw.at[0], vg0.at[z, y, 0]), local(gw.at[0], vg0.at[z, y, 1])]
    own_vg1 = [local(vw.at[1], vg1.at[z, y, 0]), local(gw.at[1], vg1.at[z, y, 1])]
    own_xs = local(stream_hbm, xs)
    own_cg = local(cgain, cg.at[tp])

    zlo, zhi = lax.rem(z, TP), lax.div(z, TP)
    far = zlo != tp
    partner = (zhi * TP + tp, y, lax.div(zlo, C), lax.rem(zlo, C))
    nsp = lax.rem(sp + 1, Z * Y)
    psp = lax.rem(sp + Z * Y - 1, Z * Y)
    after = (lax.div(nsp, Y), lax.rem(nsp, Y), x, c)
    before = (lax.div(psp, Y), lax.rem(psp, Y), x, c)

    barrier = pltpu.get_barrier_semaphore()
    peers = [(zp(d), y, x, c) for d in (1, 2, -1, -2)] + [(z, yp(d), x, c) for d in (1, -1)]
    for d in range(1, TP):
        other = lax.rem(tp + d, TP)
        peers.append((z, y, lax.div(other, C), lax.rem(other, C)))
    peers += [after, before]
    for peer in peers:
        pl.semaphore_signal(barrier, inc=1, device_id=peer, device_id_type=MESH)

    @pl.when(far)
    def _():
        pl.semaphore_signal(barrier, inc=1, device_id=partner, device_id_type=MESH)

    pl.semaphore_wait(barrier, len(peers) + jnp.where(far, 1, 0))

    z_in = {}

    def z_send(m, buf, slot, direction, d):
        dist = 1 if d % 2 else 2
        at = buf.at[slot, y]
        copy = remote(at, at, (zp(direction * dist), y, x, c))
        copy.start()
        back = buf.at[zp(-direction * d), y]
        z_in[m, direction, d] = pltpu.make_async_remote_copy(
            src_ref=back, dst_ref=back, send_sem=copy.src_sem, recv_sem=copy.dst_sem,
            device_id=(z, y, x, c), device_id_type=MESH,
        )

    def z_stage(m, buf, s):
        for direction, most in ((1, Z // 2), (-1, Z // 2 - 1)):
            slot = zp(-direction * 2 * s)
            if s:
                z_in[m, direction, 2 * s].wait_recv()
            for d in (2 * s + 2, 2 * s + 1):
                if d <= most:
                    z_send(m, buf, slot, direction, d)

    y_in = {}
    y_far = {}

    def arriving(copy, at):
        return pltpu.make_async_remote_copy(
            src_ref=at, dst_ref=at, send_sem=copy.src_sem, recv_sem=copy.dst_sem,
            device_id=(z, y, x, c), device_id_type=MESH,
        )

    def y_send(m, buf, key, rows, plus, minus):
        for direction in (1, -1):
            at = buf.at[rows, y]
            copy = remote(at, at, (z, yp(direction), x, c))
            copy.start()
            y_in[m, key, direction] = arriving(copy, buf.at[rows, yp(-direction)])

    def y_relay(m, buf, key, piece):
        for direction in (1, -1):
            y_in[m, key, direction].wait_recv()
            at = piece(direction, yp(-direction))
            copy = remote(at, at, (z, yp(direction), x, c))
            copy.start()
            y_far[m, key, direction] = arriving(copy, piece(direction, yp(-2 * direction)))

    def y_done(m, key):
        for direction in (1, -1):
            y_far[m, key, direction].wait_recv()

    def half_of_pair(buf, rows):
        return lambda direction, row: buf.at[rows, row, 0 if direction == 1 else 1]

    def half_of_rows(buf):
        return lambda direction, row: buf.at[pl.ds(0 if direction == 1 else Z // 2, Z // 2), row]

    perm = []
    for layer, buf in ((0, ou0), (1, ou1)):
        there = buf.at[zhi * TP + tp, y, 0]
        perm.append(remote(ow.at[layer], there, partner, keep=False))
    perm_sem = [new_sem() for _ in range(2)]
    gains_in = []

    for copy in own_vg0:
        copy.wait()
    z_stage("vg0", vg0, 0)
    y_send("vg0", vg0, 0, z, None, None)

    @pl.when(far)
    def _():
        for copy in perm:
            copy.start()

    @pl.when(jnp.logical_not(far))
    def _():
        for layer, buf in ((0, ou0), (1, ou1)):
            pltpu.make_async_copy(ow.at[layer], buf.at[z, y, 0], perm_sem[layer]).start()

    for copy in own_vg1:
        copy.wait()
    z_stage("vg1", vg1, 0)

    own_cg.wait()
    for d in range(1, TP):
        to, frm = lax.rem(tp + d, TP), lax.rem(tp + TP - d, TP)
        copy = remote(cg.at[tp], cg.at[tp], (z, y, lax.div(to, C), lax.rem(to, C)))
        copy.start()
        gains_in.append(arriving(copy, cg.at[frm]))

    rows_all, width = xs.shape
    cols = gx.shape[2] * 2

    def group_of(layer, g, rows):
        if layer == 0:
            return xs[rows, pl.ds(g * 128, 128)]
        return s1[g % TP, g // TP, rows, :]

    def normalise(layer):
        step = 16

        @pl.loop(0, rows_all // step)
        def _(i):
            rows = pl.ds(pl.multiple_of(i * step, step), step)
            groups = [group_of(layer, g, rows).astype(F32) for g in range(width // 128)]
            total = groups[0] * groups[0]
            for g in groups[1:]:
                total = total + g * g
            scale = lax.rsqrt(jnp.sum(total, axis=1, keepdims=True) / width + EPS)
            for g, wide in enumerate(groups):
                gain = ngain[pl.ds(layer, 1), pl.ds(g * 128, 128)]
                nb[rows, pl.ds(g * 128, 128)] = (wide * scale * gain).astype(BF16)

    def project(layer, buf, gb):
        n = nb[...]
        value = jnp.dot(n, buf[:, :, 0].reshape(width, cols), preferred_element_type=F32)
        gate = jnp.dot(n, buf[:, :, 1].reshape(width, cols), preferred_element_type=F32)
        gated = (value * sigmoid(gate)).astype(BF16)
        gb[...] = gated[rows_all - 32 :]
        wide = gated.astype(F32)
        for h in range(2):
            gx[h, 32:, :] = wide[:, h * 128 : (h + 1) * 128]

    def convolve(layer, f, block):
        n = 64
        for h in range(2):
            acc = None
            for k in range(31):
                term = taps[layer, pl.ds(k, 1), pl.ds(h * 128, 128)] * gx[h, block * n + 2 + k : block * n + 2 + k + n, :]
                acc = term if acc is None else acc + term
            f[tp, block // 2, (block % 2) * n : (block % 2) * n + n, h * 128 : (h + 1) * 128] = acc.astype(BF16)

    def halo(layer, gb, hbuf):
        copy = remote(gb, hbuf, after, keep=False)

        @pl.when(sp < Z * Y - 1)
        def _():
            copy.start()

        return copy

    def halo_arrives(copy, hbuf):
        @pl.when(sp > 0)
        def _():
            copy.wait_recv()
            for h in range(2):
                gx[h, 0:32, :] = hbuf[:, h * 128 : (h + 1) * 128].astype(F32)

        @pl.when(sp == 0)
        def _():
            gx[:, 0:32, :] = jnp.zeros((2, 32, 128), F32)

    def halo_sent(copy):
        @pl.when(sp < Z * Y - 1)
        def _():
            copy.wait_send()

    def gather_tp(buf):
        me, other = buf.at[tp], (z, y, x, 1 - c)
        mate = tp + 1 - 2 * c

        def slot(d):
            return xp(d) * C + c

        def mate_slot(d):
            return xp(d) * C + 1 - c

        direct, passed = {}, []
        for direction in (1, -1):
            copy = remote(me, me, (z, y, xp(direction), c))
            copy.start()
            direct[direction] = arriving(copy, buf.at[slot(-direction)])
        copy = remote(me, me, other)
        copy.start()
        passed.append(arriving(copy, buf.at[mate]))
        relayed = {}
        for direction, half in ((1, 0), (-1, 1)):
            direct[direction].wait_recv()
            at = buf.at[slot(-direction), half]
            copy = remote(at, at, (z, y, xp(direction), c))
            copy.start()
            relayed[direction] = arriving(copy, buf.at[slot(2), half])
            at = buf.at[slot(-direction)]
            copy = remote(at, at, other)
            copy.start()
            passed.append(arriving(copy, buf.at[mate_slot(-direction)]))
        for direction, half in ((1, 0), (-1, 1)):
            relayed[direction].wait_recv()
            at = buf.at[slot(2), half]
            copy = remote(at, at, other)
            copy.start()
            passed.append(arriving(copy, buf.at[mate_slot(2), half]))
        for copy in passed:
            copy.wait_recv()

    def activate_and_project(layer, f, ou, nxt):
        n = rows_all // 2
        for half in range(2):
            first = second = jnp.zeros((n, 128), F32)
            for k in range(TP):
                for h in range(2):
                    part = f[k, half, :, h * 128 : (h + 1) * 128].astype(F32)
                    first = first + part
                    second = second + part * part
            mean = jnp.sum(first, axis=1, keepdims=True) / width
            var = jnp.sum(second, axis=1, keepdims=True) / width - mean * mean
            scale = lax.rsqrt(var + EPS)
            total = [jnp.zeros((n, 128), F32) for _ in range(2)]
            for k in range(TP):
                v = (f[k, half].astype(F32) - mean) * scale * cg[k, pl.ds(layer, 1), :]
                act = (v * sigmoid(v)).astype(BF16)
                for hi in range(2):
                    w = ou[hi * TP + k, :, 0].reshape(128, cols)
                    total[hi] = total[hi] + lax.dot_general(
                        act, w, (((1,), (1,)), ((), ())), preferred_element_type=F32
                    )
            for hi in range(2):
                rows = pl.ds(half * n, n)
                if layer == 0:
                    lane = pl.multiple_of((hi * TP + tp) * 128, 128)
                    old = xs[rows, pl.ds(lane, 128)]
                else:
                    old = s1[tp, hi, rows, :]
                nxt[tp, hi, rows, :] = (old.astype(F32) + total[hi]).astype(BF16)

    own_xs.wait()
    normalise(0)

    def new_keys(s):
        keys = []
        for direction, most in ((1, Z // 2), (-1, Z // 2 - 1)):
            keys += [direction * d for d in (2 * s, 2 * s - 1) if d <= most]
        return keys

    def pass_on(keys):
        for key in keys:
            d = abs(key)
            direction = 1 if key > 0 else -1
            if d % 2 or d == Z // 2:
                z_in["vg0", direction, d].wait_recv()
            y_send("vg0", vg0, key, zp(-key), None, None)

    def relay(keys):
        for key in keys:
            y_relay("vg0", vg0, key, half_of_pair(vg0, zp(-key)))

    old_keys = [0]
    for s in range(1, 4):
        z_stage("vg0", vg0, s)
        keys = new_keys(s)
        pass_on(keys)
        if s == 1:
            @pl.when(far)
            def _():
                for copy in perm:
                    copy.wait_recv()

            @pl.when(jnp.logical_not(far))
            def _():
                for layer, buf in ((0, ou0), (1, ou1)):
                    pltpu.make_async_copy(ow.at[layer], buf.at[z, y, 0], perm_sem[layer]).wait()

        relay(old_keys)
        old_keys = keys
        z_stage("ou0", ou0, s - 1)
        z_stage("vg1", vg1, s)
        z_stage("ou1", ou1, s - 1)
    keys = new_keys(4)
    pass_on(keys)
    relay(old_keys)
    z_stage("ou0", ou0, 3)
    z_stage("ou1", ou1, 3)
    relay(keys)
    every = [0] + [k for s in range(1, 5) for k in new_keys(s)]

    def z_rest(m, last_waited):
        for direction, most in ((1, Z // 2), (-1, Z // 2 - 1)):
            for d in range(1, most + 1):
                if d % 2 or d > last_waited:
                    z_in[m, direction, d].wait_recv()

    z_rest("ou0", 6)
    y_send("ou0", ou0, 0, pl.ds(0, Z), None, None)
    for key in every:
        y_done("vg0", key)

    project(0, vg0, gb0)
    copy0 = halo(0, gb0, h0)
    for b in (1, 2, 3):
        convolve(0, f0, b)
    halo_arrives(copy0, h0)
    convolve(0, f0, 0)
    y_relay("ou0", ou0, 0, half_of_rows(ou0))
    z_rest("vg1", 6)
    y_send("vg1", vg1, 0, pl.ds(0, Z), None, None)
    gather_tp(f0)
    for copy in gains_in:
        copy.wait_recv()
    y_done("ou0", 0)
    activate_and_project(0, f0, ou0, s1)
    gather_tp(s1)
    normalise(1)
    y_relay("vg1", vg1, 0, half_of_pair(vg1, pl.ds(0, Z)))
    z_rest("ou1", 6)
    y_send("ou1", ou1, 0, pl.ds(0, Z), None, None)
    y_done("vg1", 0)

    project(1, vg1, gb1)
    copy1 = halo(1, gb1, h1)
    for b in (1, 2, 3):
        convolve(1, f1, b)
    halo_arrives(copy1, h1)
    convolve(1, f1, 0)
    gather_tp(f1)
    y_relay("ou1", ou1, 0, half_of_rows(ou1))
    y_done("ou1", 0)
    activate_and_project(1, f1, ou1, s2)
    gather_tp(s2)
    for g in range(width // 128):
        out_ref[:, g * 128 : (g + 1) * 128] = s2[g % TP, g // TP]

    for copy in sent:
        copy.wait_send()
    halo_sent(copy0)
    halo_sent(copy1)

    @pl.when(far)
    def _():
        for copy in perm:
            copy.wait_send()

    assert used[0] <= N_SEMS, used[0]


def body(stream_in, norm_gain, value_weight, gate_weight, conv_taps, channel_gain, out_weight):
    rows, width = stream_in.shape
    depth, cols = value_weight.shape[1:]
    any_, vmem = pl.BlockSpec(memory_space=pl.ANY), pl.BlockSpec(memory_space=pltpu.VMEM)
    out_t = jnp.swapaxes(out_weight, 1, 2)
    return pl.pallas_call(
        kernel,
        out_shape=jax.ShapeDtypeStruct((rows, width), BF16),
        in_specs=[any_, vmem, any_, any_, vmem, any_, any_],
        out_specs=vmem,
        scratch_shapes=[
            pltpu.VMEM((Z, Y, 2, depth, cols), BF16),
            pltpu.VMEM((Z, Y, 2, depth, cols), BF16),
            pltpu.VMEM((Z, Y, 1, depth, cols), BF16),
            pltpu.VMEM((Z, Y, 1, depth, cols), BF16),
            pltpu.VMEM((rows, width), BF16),
            pltpu.VMEM((TP, 2, rows, 128), BF16),
            pltpu.VMEM((TP, 2, rows, 128), BF16),
            pltpu.VMEM((TP, 2, rows // 2, cols), BF16),
            pltpu.VMEM((TP, 2, rows // 2, cols), BF16),
            pltpu.VMEM((rows, width), BF16),
            pltpu.VMEM((2, rows + 32, 128), F32),
            pltpu.VMEM((32, cols), BF16),
            pltpu.VMEM((32, cols), BF16),
            pltpu.VMEM((32, cols), BF16),
            pltpu.VMEM((32, cols), BF16),
            pltpu.VMEM((TP, 2, cols), F32),
            pltpu.SemaphoreType.DMA((N_SEMS,)),
        ],
        compiler_params=pltpu.CompilerParams(
            collective_id=0, has_side_effects=True, vmem_limit_bytes=48 * 1024 * 1024
        ),
    )(stream_in, norm_gain, value_weight, gate_weight, conv_taps, channel_gain, out_t)


def solution(mesh):
    finer = Mesh(mesh.devices.reshape(Z, Y, X, C), ("z", "y", "x", "c"))
    sp, tp = ("z", "y"), ("x", "c")
    placed = (
        P(sp, None),
        P(),
        P(None, sp, tp),
        P(None, sp, tp),
        P(None, None, tp),
        P(None, tp),
        P(None, tp, sp),
    )
    return jax.shard_map(body, mesh=finer, in_specs=placed, out_specs=P(sp, None), check_vma=False)
```

time: 484 us -> 123 us (0.25)
  waiting for transfers between devices: 310 us -> 0 us
  Pallas kernels: 0 us -> 119 us
  blocking collectives: 90.1 us -> 0 us
  starting transfers between devices: 40 us -> 0 us
  between operations: 13.3 us -> 0.07 us
  matrix products: 10.8 us -> 0 us
  other arithmetic: 9.64 us -> 0 us
  local copies, waits for them, and re-layouts: 8.66 us -> 3.1 us
    all_gather x4 -> x0, waiting for transfers between devices: 288 us -> none  [the longest x2 207 us: side_by_side(): out = lax.all_gather(both, axis, axis=dim, tiled=True)]
    pallas_call x0 -> x1, Pallas kernels: none -> 119 us  [body(): pl.pallas_call(kernel, out_shape=jax.ShapeDtypeStruct((rows, width), BF16...]
    all_to_all x3 -> x0, blocking collectives: 68.5 us -> none  [the longest x2 38.2 us: sent_to_all(): return lax.all_to_all(copies, axis, split_axis=0, concat_axis=0, tiled=True)]
    all_to_all x3 -> x0, starting transfers between devices: 35.4 us -> none  [the longest x2 19.8 us: sent_to_all(): return lax.all_to_all(copies, axis, split_axis=0, concat_axis=0, tiled=True)]
    all_to_all x3 -> x0, waiting for transfers between devices: 22.5 us -> none  [the longest x1 13.4 us: summed_on_arrival(): parts = lax.all_to_all(in_blocks(shard, dim, peers), axis, 0, 0, tiled=True)]
    all_gather x2 -> x0, blocking collectives: 21.6 us -> none  [gathered_by_axis(): nearer = lax.all_gather(shard, axes[-1], axis=dim, tiled=True)]
    dot_general x6 -> x0, matrix products: 10.8 us -> none  [the longest x2 4.42 us: body(): jnp.dot(activated, full_out, preferred_element_type=jnp.float32)]
    slice x9 -> x0, local copies, waits for them, and re-layouts: 4.97 us -> none  [the longest x4 3.4 us: body(): filtered = filtered + taps[tap] * padded[tap:tap + tok_rows]]
  transfers between devices with their start and end apart: 9 -> 0, of which waited for: 8 -> 0; matrix products, arithmetic and copies ran while one was open for 5% -> 0% of each run, Pallas kernels for 0% -> 0%
where the time goes in v1:
time: 123 us; the launch traced here: 122 us
  Pallas kernels  119 us (97%)
  local copies, waits for them, and re-layouts  3.1 us (3%)
    pallas_call x1, Pallas kernels, body(): pl.pallas_call(kernel, out_shape=jax.ShapeDtypeStruct((rows, width), BF16...  119 us
    unnamed x14, local copies, waits for them, and re-layouts  3.1 us

profile of v1, /device:TPU:1, one launch (start us, length us, event | category | flops | bytes accessed | tf_op | source)
XLA Modules:
  0.0 122.2 jit_solution(17273234540380102640)
XLA Ops:
  0.0 0.0 copy-start.1
  0.0 0.0 copy-start.2
  0.0 0.0 copy-start.3
  0.0 0.0 copy-start.4
  0.0 0.0 copy-start.5
  0.0 0.9 copy.8.taps
  0.9 0.0 copy-done.1
  0.9 0.0 copy-done.2
  0.9 0.0 copy-done.3
  0.9 0.0 copy-done.4
  0.9 0.0 copy-done.5
  1.0 0.0 copy-start
  1.0 1.2 copy-done
  2.2 119.1 %shard_map.73 = bf16[256,2048]{1,0:T(8,128)(2,1)S(1)} custom-call(bf16[256,2048]{1,0:T(8,128)(2,1)S(1)} %copy-done, f32[2,2048]{1,0:T(2,128)S(1)} %copy-done.4, bf16[2,32,256]{2,1,0:T(8,128)(2,1)S(1)} %copy-done.1, bf16[2,32,256]{2,1,0:T(8,128)(2,1)S(1)} %copy-done.2, f32[2,31,256]{2,1,0:T(8,128)S(1)} %copy.8.taps, f32[2,256]{1,0:T(2,128)S(1)} %copy-done.5, ...), custom_call_target="tpu_custom_call" | custom-call | tf_op jit(solution)/shard_map/pallas_call | solution.py:426
  121.3 1.0 copy.10
Async XLA Ops:
  0.0 0.9 copy-start.1
  0.0 0.9 copy-start.2
  0.0 0.9 copy-start.3
  0.0 0.9 copy-start.4
  0.0 0.9 copy-start.5
  1.0 1.2 %copy-start = (bf16[256,2048]{1,0:T(8,128)(2,1)S(1)}, bf16[256,2048]{1,0:T(8,128)(2,1)}, u32[]{:S(2)}) copy-start(bf16[256,2048]{1,0:T(8,128)(2,1)} %stream_hbm.1) | copy-start | bytes 3145732

commit v2 on v0

v2 whole, which is shorter than its diff:
```python
import jax
import jax.numpy as jnp
from jax import lax
from jax.experimental import pallas as pl
from jax.experimental.pallas import tpu as pltpu
from jax.sharding import Mesh
from jax.sharding import PartitionSpec as P

Z, Y, X, C = 16, 4, 4, 2
TP = X * C
MESH = pl.DeviceIdType.MESH
EPS = 1e-05
F32 = jnp.float32
BF16 = jnp.bfloat16
N_SEMS = 106
HALO = 32
RING = [
    [(2 * s, tuple(d for d in (2 * s + 2, 2 * s + 1) if d <= Z // 2)),
     (-2 * s, tuple(-d for d in (2 * s + 2, 2 * s + 1) if d < Z // 2))]
    for s in range(4)
]
VMEM_LIMIT = 67043328
scope = jax.named_scope


def sigmoid(v):
    return 0.5 + 0.5 * jnp.tanh(0.5 * v)


def kernel(
    stream_hbm, ngain, vw, gw, taps, cgain, ow, out_ref,
    vg0, vg1, ou0, ou1, xs, s1, s2, f0, f1, nb, gx, h0, h1, gb0, gb1, cg, sems,
):
    z, y, x, c = (lax.axis_index(a) for a in ("z", "y", "x", "c"))
    tp = x * C + c
    sp = z * Y + y
    used = [0]

    def new_sem():
        used[0] += 1
        return sems.at[used[0] - 1]

    def send(src, dst, device, send_sem, recv_sem):
        pltpu.make_async_remote_copy(
            src_ref=src, dst_ref=dst, send_sem=send_sem, recv_sem=recv_sem,
            device_id=device, device_id_type=MESH,
        ).start()

    def wait(ref, sem):
        pltpu.make_async_copy(ref, ref, sem).wait()

    drains = []

    def send_group(ref):
        sem = new_sem()
        drains.append((ref, sem))
        return sem

    def zp(d):
        return lax.rem(z + d + Z, Z)

    def yp(d):
        return lax.rem(y + d + Y, Y)

    def xp(d):
        return lax.rem(x + d + X, X)

    own_sem = [new_sem() for _ in range(4)]
    own = [
        pltpu.make_async_copy(vw.at[0], vg0.at[z, y, 0], own_sem[0]),
        pltpu.make_async_copy(gw.at[0], vg0.at[z, y, 1], own_sem[0]),
        pltpu.make_async_copy(vw.at[1], vg1.at[z, y, 0], own_sem[1]),
        pltpu.make_async_copy(gw.at[1], vg1.at[z, y, 1], own_sem[1]),
        pltpu.make_async_copy(stream_hbm, xs, own_sem[2]),
        pltpu.make_async_copy(cgain, cg.at[tp], own_sem[3]),
    ]
    for copy in own:
        copy.start()

    zlo, zhi = lax.rem(z, TP), lax.div(z, TP)
    far = zlo != tp
    partner = (zhi * TP + tp, y, lax.div(zlo, C), lax.rem(zlo, C))
    nsp = lax.rem(sp + 1, Z * Y)
    psp = lax.rem(sp + Z * Y - 1, Z * Y)
    after = (lax.div(nsp, Y), lax.rem(nsp, Y), x, c)
    before = (lax.div(psp, Y), lax.rem(psp, Y), x, c)

    barrier = pltpu.get_barrier_semaphore()
    peers = [(zp(d), y, x, c) for d in (1, 2, -1, -2)] + [(z, yp(d), x, c) for d in (1, -1, 2)]
    for d in range(1, TP):
        other = lax.rem(tp + d, TP)
        peers.append((z, y, lax.div(other, C), lax.rem(other, C)))
    peers += [after, before]
    for peer in peers:
        pl.semaphore_signal(barrier, inc=1, device_id=peer, device_id_type=MESH)

    @pl.when(far)
    def _():
        pl.semaphore_signal(barrier, inc=1, device_id=partner, device_id_type=MESH)

    with scope("barrier"):
        pl.semaphore_wait(barrier, len(peers) + jnp.where(far, 1, 0))

    z_sems = {}

    def brought(plan, s):
        return [d for _, news in plan[s] for d in news]

    def z_block(buf, slot, part):
        return buf.at[slot, y] if part is None else buf.at[slot, y, part]

    def z_stage(m, buf, plan, s, part=None):
        if s == 0:
            z_sems[m, part] = [new_sem() for _ in plan], send_group(z_blocks(buf, Z - 1, part))
        sems_in, out = z_sems[m, part]
        for d, news in plan[s]:
            at = z_block(buf, zp(-d), part)
            for new in news:
                send(at, at, (zp(new - d), y, x, c), out, sems_in[s])

    def z_blocks(buf, n, part):
        return buf.at[pl.ds(0, n), 0] if part is None else buf.at[pl.ds(0, n), 0, part]

    def z_wait(m, buf, plan, s, part=None):
        wait(z_blocks(buf, len(brought(plan, s)), part), z_sems[m, part][0][s])

    y_sems = {}

    def y_group(m, buf):
        pair = buf.shape[2] == 2
        sent, passed = send_group(buf.at[:, pl.ds(0, 2)]), send_group(buf.at[:, 0])
        y_sems[m] = sent, passed, new_sem(), {}

        def half(slot, row, h):
            return buf.at[slot, row, h] if pair else buf.at[slot, row, 0, pl.ds(h * 16, 16)]

        def pass_on(key, ds):
            first, second = new_sem(), new_sem()
            y_sems[m][3][key] = first, second
            for d in ds:
                at = buf.at[zp(-d), y]
                send(at, at, (z, yp(1), x, c), sent, first)
                send(at, at, (z, yp(-1), x, c), sent, second)

        def relay(key, ds):
            for direction, h, sem in ((1, 0, y_sems[m][3][key][0]), (-1, 1, y_sems[m][3][key][1])):
                wait(buf.at[pl.ds(0, len(ds)), 0], sem)
                for d in ds:
                    at = half(zp(-d), yp(-direction), h)
                    send(at, at, (z, yp(direction), x, c), passed, y_sems[m][2])

        def pass_far(key, ds):
            pass_on(key, ds)
            for d in ds:
                at = buf.at[zp(-d), y]
                send(at, at, (z, yp(2), x, c), passed, y_sems[m][2])

        def near_done(key, ds):
            for sem in y_sems[m][3][key]:
                wait(buf.at[pl.ds(0, len(ds)), 0], sem)

        def done():
            wait(buf.at[:, 0], y_sems[m][2])

        return pass_on, relay, pass_far, near_done, done

    mine = lax.rem(z, 2)

    def spread(m, buf):
        pair = buf.shape[2] == 2
        quarter = pl.ds(0, Z // 2)
        whole = buf.at[:, 0, 0] if pair else buf.at[quarter, 0, 0]
        part_half = buf.at[quarter, 0, 0] if pair else buf.at[pl.ds(0, Z // 4), 0, 0]
        all3 = buf.at[:, pl.ds(0, 3), 0] if pair else buf.at[quarter, pl.ds(0, 3), 0]
        sent = send_group(buf.at[:, 0] if pair else buf.at[:, 0, 0])
        passed = send_group(whole)
        swapped = send_group(all3)
        row_in, far_in, swap_in = [new_sem(), new_sem()], [new_sem(), new_sem()], new_sem()
        ways = ((1, 0), (-1, 1))

        def piece(row, part, half=None):
            if pair:
                n = Z if half is None else Z // 2
                return buf.at[pl.ds((half or 0) * Z // 2, n), row, part]
            n = Z // 2 if half is None else Z // 4
            return buf.at[pl.ds(part * (Z // 2) + (half or 0) * Z // 4, n), row, 0]

        def a():
            for direction, h in ways:
                send(piece(y, mine), piece(y, mine), (z, yp(direction), x, c), sent, row_in[h])

        def b():
            for direction, h in ways:
                wait(whole, row_in[h])
                at = piece(yp(-direction), mine, h)
                send(at, at, (z, yp(direction), x, c), passed, far_in[h])
            for direction, h in ways:
                at = piece(yp(-direction), mine)
                send(at, at, (zp(direction), y, x, c), swapped, swap_in)

        def e():
            for direction, h in ways:
                wait(part_half, far_in[h])
                at = piece(yp(2), mine, h)
                send(at, at, (zp(direction), y, x, c), swapped, swap_in)

        def done():
            wait(all3, swap_in)

        return a, b, e, done

    def gather_tp(buf, h):
        me, other = buf.at[tp, h], (z, y, x, 1 - c)
        out = send_group(buf.at[pl.ds(0, TP - 1), h])
        near_in, far_in, mate = new_sem(), new_sem(), new_sem()

        def slot(d):
            return buf.at[xp(d) * C + c, h]

        def begin():
            for d, sem in ((2, far_in), (1, near_in), (-1, near_in)):
                send(me, me, (z, y, xp(d), c), out, sem)
            send(me, me, other, out, mate)

        def near():
            wait(buf.at[pl.ds(0, 2), h], near_in)
            for d in (1, -1):
                send(slot(d), slot(d), other, out, mate)

        def last():
            wait(me, far_in)
            send(slot(2), slot(2), other, out, mate)

        def done():
            wait(buf.at[pl.ds(0, X), h], mate)

        return begin, near, last, done

    rows_all, width = xs.shape
    cols = gx.shape[2] * 2
    nh = rows_all // 2

    def normalise(layer, h):
        n = 64
        for i in range(nh // n):
            rows = pl.ds(h * nh + i * n, n)

            def group(g):
                if layer == 0:
                    return xs[rows, pl.ds(g * 128, 128)].astype(F32)
                return s1[g % TP, h, g // TP, pl.ds(i * n, n), :].astype(F32)

            total = None
            for g in range(width // 128):
                wide = group(g)
                total = wide * wide if total is None else total + wide * wide
            scale = lax.rsqrt(jnp.sum(total, axis=1, keepdims=True) / width + EPS)
            for g in range(width // 128):
                gain = ngain[pl.ds(layer, 1), pl.ds(g * 128, 128)]
                nb[rows, pl.ds(g * 128, 128)] = (group(g) * scale * gain).astype(BF16)

    def project(layer, buf, gb, h):
        n = nb[pl.ds(h * nh, nh), :]
        value = jnp.dot(n, buf[:, :, 0].reshape(width, cols), preferred_element_type=F32)
        gate = jnp.dot(n, buf[:, :, 1].reshape(width, cols), preferred_element_type=F32)
        gated = (value * sigmoid(gate)).astype(BF16)
        if h:
            gb[...] = gated[nh - HALO :]
        wide = gated.astype(F32)
        for j in range(2):
            gx[j, HALO + h * nh : HALO + h * nh + nh, :] = wide[:, j * 128 : (j + 1) * 128]

    def convolve(layer, f, block):
        n = 64
        first = block * n + HALO - 30
        for j in range(2):
            acc = None
            for k in range(31):
                term = taps[k, pl.ds(layer, 1), pl.ds(j * 128, 128)] * gx[j, first + k : first + k + n, :]
                acc = term if acc is None else acc + term
            f[tp, block // 2, (block % 2) * n : (block % 2) * n + n, j * 128 : (j + 1) * 128] = acc.astype(BF16)

    def halo(gb, hbuf):
        copy = pltpu.make_async_remote_copy(
            src_ref=gb, dst_ref=hbuf, send_sem=new_sem(), recv_sem=new_sem(),
            device_id=after, device_id_type=MESH,
        )

        @pl.when(sp < Z * Y - 1)
        def _():
            copy.start()

        def arrives():
            @pl.when(sp > 0)
            def _():
                copy.wait_recv()
                for j in range(2):
                    gx[j, 0:HALO, :] = hbuf[:, j * 128 : (j + 1) * 128].astype(F32)

            @pl.when(sp == 0)
            def _():
                gx[:, 0:HALO, :] = jnp.zeros((2, HALO, 128), F32)

        def sent():
            @pl.when(sp < Z * Y - 1)
            def _():
                copy.wait_send()

        return arrives, sent

    def activate_and_project(layer, f, ou, nxt, h):
        first = second = jnp.zeros((nh, 128), F32)
        for k in range(TP):
            for j in range(2):
                part = f[k, h, :, j * 128 : (j + 1) * 128].astype(F32)
                first = first + part
                second = second + part * part
        mean = jnp.sum(first, axis=1, keepdims=True) / width
        var = jnp.sum(second, axis=1, keepdims=True) / width - mean * mean
        scale = lax.rsqrt(var + EPS)
        total = [jnp.zeros((nh, 128), F32) for _ in range(2)]
        for k in range(TP):
            v = (f[k, h].astype(F32) - mean) * scale * cg[k, pl.ds(layer, 1), :]
            act = (v * sigmoid(v)).astype(BF16)
            for hi in range(2):
                w = ou[hi * TP + k, :, 0].reshape(128, cols)
                total[hi] = total[hi] + lax.dot_general(
                    act, w, (((1,), (1,)), ((), ())), preferred_element_type=F32
                )
        for hi in range(2):
            if layer == 0:
                lane = pl.multiple_of((hi * TP + tp) * 128, 128)
                old = xs[pl.ds(h * nh, nh), pl.ds(lane, 128)]
            else:
                old = s1[tp, h, hi]
            nxt[tp, h, hi] = (old.astype(F32) + total[hi]).astype(BF16)

    perm_send = send_group(ow)
    perm_recv = new_sem()
    perm = [
        pltpu.make_async_remote_copy(
            src_ref=ow.at[layer], dst_ref=buf.at[zhi * TP + tp, y, 0], send_sem=perm_send, recv_sem=perm_recv,
            device_id=partner, device_id_type=MESH,
        )
        for layer, buf in ((0, ou0), (1, ou1))
    ]
    drains.pop()
    stay = [pltpu.make_async_copy(ow.at[layer], buf.at[z, y, 0], perm_recv) for layer, buf in ((0, ou0), (1, ou1))]

    def perm_start():
        @pl.when(far)
        def _():
            for copy in perm:
                copy.start()

        @pl.when(jnp.logical_not(far))
        def _():
            for copy in stay:
                copy.start()

    def perm_done():
        wait(ow, perm_recv)

    pass_vg, relay_vg, far_vg, near_vg, done_vg = y_group("vg0", vg0)
    ou0_a, ou0_b, ou0_c, ou0_done = spread("ou0", ou0)
    vg1_a, vg1_b, vg1_c, vg1_done = spread("vg1", vg1)
    ou1_a, ou1_b, ou1_c, ou1_done = spread("ou1", ou1)

    def vg0_stage(s):
        for part in range(2):
            if s:
                z_wait("vg0", vg0, RING, s - 1, part)
            if s < 4:
                z_stage("vg0", vg0, RING, s, part)

    wait(vg0.at[z, y], own_sem[0])
    vg0_stage(0)
    pass_vg(0, [0])
    perm_start()
    wait(vg1.at[z, y], own_sem[1])
    z_stage("vg1", vg1, RING, 0)
    wait(cg.at[tp], own_sem[3])
    gain_sent, gain_in = send_group(cg.at[pl.ds(0, TP - 1)]), new_sem()
    for d in range(1, TP):
        to = lax.rem(tp + d, TP)
        send(cg.at[tp], cg.at[tp], (z, y, lax.div(to, C), lax.rem(to, C)), gain_sent, gain_in)
    wait(xs, own_sem[2])
    with scope("norm0"):
        for h in range(2):
            normalise(0, h)

    ring = [[0]] + [brought(RING, s) for s in range(4)]

    def ring_step(m, buf, s):
        z_wait(m, buf, RING, s - 1)
        if s < 4:
            z_stage(m, buf, RING, s)

    with scope("stage1"):
        vg0_stage(1)
        pass_vg(1, ring[1])
        relay_vg(0, ring[0])
    with scope("stage2"):
        vg0_stage(2)
        pass_vg(2, ring[2])
        relay_vg(1, ring[1])
        perm_done()
        z_stage("ou0", ou0, RING, 0)
        ring_step("vg1", vg1, 1)
    with scope("stage3"):
        vg0_stage(3)
        pass_vg(3, ring[3])
        relay_vg(2, ring[2])
        ring_step("ou0", ou0, 1)
        ring_step("vg1", vg1, 2)
    with scope("stage4"):
        vg0_stage(4)
        far_vg(4, ring[4])
        relay_vg(3, ring[3])
        ring_step("ou0", ou0, 2)
        ring_step("vg1", vg1, 3)
        z_stage("ou1", ou1, RING, 0)
    with scope("stage5"):
        ring_step("ou0", ou0, 3)
    with scope("vg0done"):
        near_vg(4, ring[4])
        done_vg()

    def layer_head(layer, vg, gb, hbuf, f, ready):
        first, second = gather_tp(f, 1), gather_tp(f, 0)
        with scope("proj"):
            project(layer, vg, gb, 1)
        arrives, sent = halo(gb, hbuf)
        with scope("projb"):
            ready()
            project(layer, vg, gb, 0)
        with scope("conv"):
            convolve(layer, f, 2)
            convolve(layer, f, 3)
        first[0]()
        with scope("convb"):
            convolve(layer, f, 1)
        return first, second, arrives, sent

    def layer_tail(layer, f, ou, nxt, parts, arrives, hooks):
        first, second = parts
        with scope("hook0"):
            hooks[0]()
        with scope("halo"):
            arrives()
            convolve(layer, f, 0)
        second[0]()
        with scope("hook0b"):
            hooks[1]()
        with scope("ag1"):
            first[1]()
            second[1]()
        with scope("hook1"):
            hooks[2]()
        with scope("ag1b"):
            first[2]()
            first[3]()
        with scope("hook2"):
            hooks[3]()
        first2, second2 = gather_tp(nxt, 1), gather_tp(nxt, 0)
        with scope("act"):
            activate_and_project(layer, f, ou, nxt, 1)
        first2[0]()
        with scope("ag1c"):
            second[2]()
            second[3]()
        with scope("actb"):
            activate_and_project(layer, f, ou, nxt, 0)
        second2[0]()
        with scope("hook3"):
            hooks[4]()
        with scope("ag2"):
            first2[1]()
            second2[1]()
        with scope("hook4"):
            hooks[5]()
        with scope("ag2b"):
            first2[2]()
            first2[3]()
        return second2

    def nothing():
        pass

    first, second, arrives, sent0 = layer_head(0, vg0, gb0, h0, f0, nothing)

    def hook00():
        ring_step("ou0", ou0, 4)
        ou0_a()
        ring_step("vg1", vg1, 4)
        vg1_a()
        ring_step("ou1", ou1, 1)

    def hook00b():
        ring_step("ou1", ou1, 2)
        ou0_b()

    def hook01():
        ou0_c()
        ring_step("ou1", ou1, 3)

    def hook02():
        vg1_b()
        wait(cg.at[pl.ds(0, TP - 1)], gain_in)
        ou0_done()

    def hook03():
        ring_step("ou1", ou1, 4)
        vg1_c()
        ou1_a()

    rest = layer_tail(0, f0, ou0, s1, (first, second), arrives, (hook00, hook00b, hook01, hook02, hook03, nothing))
    with scope("norm1"):
        normalise(1, 1)

    def ready():
        with scope("ag2c"):
            rest[2]()
            rest[3]()
        normalise(1, 0)

    with scope("vg1done"):
        vg1_done()

    first, second, arrives, sent1 = layer_head(1, vg1, gb1, h1, f1, ready)
    rest1 = layer_tail(
        1, f1, ou1, s2, (first, second), arrives, (nothing, ou1_b, ou1_c, ou1_done, nothing, nothing)
    )

    def write(h):
        for g in range(width // 128):
            out_ref[h * nh : (h + 1) * nh, g * 128 : (g + 1) * 128] = s2[g % TP, h, g // TP]

    write(1)
    with scope("ag2c"):
        rest1[2]()
        rest1[3]()
    write(0)

    with scope("out"):
        for ref, sem in drains:
            wait(ref, sem)
        sent0()
        sent1()

        @pl.when(far)
        def _():
            wait(ow, perm_send)

    assert used[0] == N_SEMS, used[0]


def body(stream_in, norm_gain, value_weight, gate_weight, conv_taps, channel_gain, out_weight):
    rows, width = stream_in.shape
    depth, cols = value_weight.shape[1:]
    hbm, vmem = pl.BlockSpec(memory_space=pltpu.HBM), pl.BlockSpec(memory_space=pltpu.VMEM)
    out_t = jnp.swapaxes(out_weight, 1, 2)
    taps = jnp.swapaxes(conv_taps, 0, 1)
    return pl.pallas_call(
        kernel,
        out_shape=jax.ShapeDtypeStruct((rows, width), BF16),
        in_specs=[hbm, vmem, hbm, hbm, vmem, hbm, hbm],
        out_specs=vmem,
        scratch_shapes=[
            pltpu.VMEM((Z, Y, 2, depth, cols), BF16),
            pltpu.VMEM((Z, Y, 2, depth, cols), BF16),
            pltpu.VMEM((Z, Y, 1, depth, cols), BF16),
            pltpu.VMEM((Z, Y, 1, depth, cols), BF16),
            pltpu.VMEM((rows, width), BF16),
            pltpu.VMEM((TP, 2, 2, rows // 2, 128), BF16),
            pltpu.VMEM((TP, 2, 2, rows // 2, 128), BF16),
            pltpu.VMEM((TP, 2, rows // 2, cols), BF16),
            pltpu.VMEM((TP, 2, rows // 2, cols), BF16),
            pltpu.VMEM((rows, width), BF16),
            pltpu.VMEM((2, rows + HALO, 128), F32),
            pltpu.VMEM((HALO, cols), BF16),
            pltpu.VMEM((HALO, cols), BF16),
            pltpu.VMEM((HALO, cols), BF16),
            pltpu.VMEM((HALO, cols), BF16),
            pltpu.VMEM((TP, 2, cols), F32),
            pltpu.SemaphoreType.DMA((N_SEMS,)),
        ],
        compiler_params=pltpu.CompilerParams(
            collective_id=0, has_side_effects=True, vmem_limit_bytes=VMEM_LIMIT
        ),
    )(stream_in, norm_gain, value_weight, gate_weight, taps, channel_gain, out_t)


def solution(mesh):
    finer = Mesh(mesh.devices.reshape(Z, Y, X, C), ("z", "y", "x", "c"))
    sp, tp = ("z", "y"), ("x", "c")
    placed = (
        P(sp, None),
        P(),
        P(None, sp, tp),
        P(None, sp, tp),
        P(None, None, tp),
        P(None, tp),
        P(None, tp, sp),
    )
    return jax.shard_map(body, mesh=finer, in_specs=placed, out_specs=P(sp, None), check_vma=False)
```

time: 484 us -> 98.3 us (0.20)
  waiting for transfers between devices: 310 us -> 0 us
  Pallas kernels: 0 us -> 95.7 us
  blocking collectives: 90.1 us -> 0 us
  starting transfers between devices: 40 us -> 0 us
  between operations: 13.3 us -> 0.01 us
  matrix products: 10.8 us -> 0 us
  other arithmetic: 9.64 us -> 0 us
  local copies, waits for them, and re-layouts: 8.66 us -> 2.3 us
    all_gather x4 -> x0, waiting for transfers between devices: 288 us -> none  [the longest x2 207 us: side_by_side(): out = lax.all_gather(both, axis, axis=dim, tiled=True)]
    pallas_call x0 -> x1, Pallas kernels: none -> 95.7 us  [body(): pl.pallas_call(kernel, out_shape=jax.ShapeDtypeStruct((rows, width), BF16...]
    all_to_all x3 -> x0, blocking collectives: 68.5 us -> none  [the longest x2 38.2 us: sent_to_all(): return lax.all_to_all(copies, axis, split_axis=0, concat_axis=0, tiled=True)]
    all_to_all x3 -> x0, starting transfers between devices: 35.4 us -> none  [the longest x2 19.8 us: sent_to_all(): return lax.all_to_all(copies, axis, split_axis=0, concat_axis=0, tiled=True)]
    all_to_all x3 -> x0, waiting for transfers between devices: 22.5 us -> none  [the longest x1 13.4 us: summed_on_arrival(): parts = lax.all_to_all(in_blocks(shard, dim, peers), axis, 0, 0, tiled=True)]
    all_gather x2 -> x0, blocking collectives: 21.6 us -> none  [gathered_by_axis(): nearer = lax.all_gather(shard, axes[-1], axis=dim, tiled=True)]
    dot_general x6 -> x0, matrix products: 10.8 us -> none  [the longest x2 4.42 us: body(): jnp.dot(activated, full_out, preferred_element_type=jnp.float32)]
    slice x9 -> x0, local copies, waits for them, and re-layouts: 4.97 us -> none  [the longest x4 3.4 us: body(): filtered = filtered + taps[tap] * padded[tap:tap + tok_rows]]
  transfers between devices with their start and end apart: 9 -> 0, of which waited for: 8 -> 0; matrix products, arithmetic and copies ran while one was open for 5% -> 0% of each run, Pallas kernels for 0% -> 0%
where the time goes in v2:
time: 98.3 us; the launch traced here: 98.1 us
  Pallas kernels  95.7 us (97%)
  local copies, waits for them, and re-layouts  2.3 us (2%)
    pallas_call x1, Pallas kernels, body(): pl.pallas_call(kernel, out_shape=jax.ShapeDtypeStruct((rows, width), BF16...  95.7 us
    unnamed x1, local copies, waits for them, and re-layouts  2.3 us

profile of v2, /device:TPU:1, one launch (start us, length us, event | category | flops | bytes accessed | tf_op | source)
XLA Modules:
  0.0 98.1 jit_solution(6193152206351565604)
XLA Ops:
  0.0 95.7 %shard_map.73 = bf16[256,2048]{1,0:T(8,128)(2,1)} custom-call(bf16[256,2048]{1,0:T(8,128)(2,1)} %stream_hbm.1, f32[2,2048]{1,0:T(2,128)} %ngain.1, bf16[2,32,256]{2,1,0:T(8,128)(2,1)} %vw.1, bf16[2,32,256]{2,1,0:T(8,128)(2,1)} %gw.1, f32[31,2,256]{2,1,0:T(2,128)} %bitcast.2, f32[2,256]{1,0:T(2,128)} %cgain.1, bf16[2,32,256]{2,1,0:T(8,128)(2,1)} %bitcast.3), custom_call_target="tpu_custom_call" | custom-call | tf_op jit(solution)/shard_map/pallas_call | solution.py:564
  95.8 2.3 %copy.9 = bf16[256,2048]{1,0:T(8,128)(2,1)} copy(bf16[256,2048]{1,0:T(8,128)(2,1)} %shard_map.73) | data formatting | bytes 2097152

commit v3 on v2

--- a/solution.py
+++ b/solution.py
@@ -12,14 +12,14 @@
 EPS = 1e-05
 F32 = jnp.float32
 BF16 = jnp.bfloat16
-N_SEMS = 106
+N_SEMS = 113
 HALO = 32
 RING = [
     [(2 * s, tuple(d for d in (2 * s + 2, 2 * s + 1) if d <= Z // 2)),
      (-2 * s, tuple(-d for d in (2 * s + 2, 2 * s + 1) if d < Z // 2))]
     for s in range(4)
 ]
-VMEM_LIMIT = 67043328
+VMEM_LIMIT = 60_000_000
 scope = jax.named_scope
 
 
@@ -77,9 +77,12 @@
     for copy in own:
         copy.start()
 
-    zlo, zhi = lax.rem(z, TP), lax.div(z, TP)
+    zlo = lax.rem(z, TP)
     far = zlo != tp
-    partner = (zhi * TP + tp, y, lax.div(zlo, C), lax.rem(zlo, C))
+    to_z = zp(lax.rem(tp - zlo + 12, TP) - 4)
+    from_z = zp(4 - lax.rem(zlo - tp + 12, TP))
+    goes_to = (to_z, y, lax.div(zlo, C), lax.rem(zlo, C))
+    comes_from = (from_z, y, lax.div(zlo, C), lax.rem(zlo, C))
     nsp = lax.rem(sp + 1, Z * Y)
     psp = lax.rem(sp + Z * Y - 1, Z * Y)
     after = (lax.div(nsp, Y), lax.rem(nsp, Y), x, c)
@@ -96,94 +99,109 @@
 
     @pl.when(far)
     def _():
-        pl.semaphore_signal(barrier, inc=1, device_id=partner, device_id_type=MESH)
+        pl.semaphore_signal(barrier, inc=1, device_id=comes_from, device_id_type=MESH)
 
     with scope("barrier"):
         pl.semaphore_wait(barrier, len(peers) + jnp.where(far, 1, 0))
 
+    def block(buf, slot, row, part=None):
+        if buf.shape[0] != Z:
+            return buf.at[lax.div(slot, 2), lax.rem(slot, 2), row]
+        return buf.at[slot, row] if part is None else buf.at[slot, row, part]
+
+    def blocks(buf, n, part=None):
+        if buf.shape[0] != Z:
+            return buf.at[pl.ds(0, max(1, n // 3)), 0, pl.ds(0, 3)] if n % 3 == 0 else buf.at[pl.ds(0, 1), 0, pl.ds(0, n)]
+        return buf.at[pl.ds(0, n), 0] if part is None else buf.at[pl.ds(0, n), 0, part]
+
     z_sems = {}
 
     def brought(plan, s):
         return [d for _, news in plan[s] for d in news]
 
-    def z_block(buf, slot, part):
-        return buf.at[slot, y] if part is None else buf.at[slot, y, part]
-
     def z_stage(m, buf, plan, s, part=None):
         if s == 0:
-            z_sems[m, part] = [new_sem() for _ in plan], send_group(z_blocks(buf, Z - 1, part))
+            z_sems[m, part] = [new_sem() for _ in plan], send_group(blocks(buf, Z - 1, part))
         sems_in, out = z_sems[m, part]
         for d, news in plan[s]:
-            at = z_block(buf, zp(-d), part)
+            at = block(buf, zp(-d), y, part)
             for new in news:
                 send(at, at, (zp(new - d), y, x, c), out, sems_in[s])
 
-    def z_blocks(buf, n, part):
-        return buf.at[pl.ds(0, n), 0] if part is None else buf.at[pl.ds(0, n), 0, part]
-
     def z_wait(m, buf, plan, s, part=None):
-        wait(z_blocks(buf, len(brought(plan, s)), part), z_sems[m, part][0][s])
-
-    y_sems = {}
+        wait(blocks(buf, len(brought(plan, s)), part), z_sems[m, part][0][s])
 
     def y_group(m, buf):
-        pair = buf.shape[2] == 2
-        sent, passed = send_group(buf.at[:, pl.ds(0, 2)]), send_group(buf.at[:, 0])
-        y_sems[m] = sent, passed, new_sem(), {}
+        pair = buf.shape[0] == Z
+        sent = send_group(buf.at[:, pl.ds(0, 2)] if pair else buf.at[pl.ds(0, 4), 0])
+        far_bytes = buf.at[:, 0] if pair else buf.at[pl.ds(0, 2), 0]
+        passed, far_in, near_in = send_group(far_bytes), new_sem(), {}
 
         def half(slot, row, h):
-            return buf.at[slot, row, h] if pair else buf.at[slot, row, 0, pl.ds(h * 16, 16)]
+            return buf.at[slot, row, h] if pair else block(buf, slot, row).at[pl.ds(h * 16, 16)]
 
         def pass_on(key, ds):
-            first, second = new_sem(), new_sem()
-            y_sems[m][3][key] = first, second
+            near_in[key] = new_sem(), new_sem()
             for d in ds:
-                at = buf.at[zp(-d), y]
-                send(at, at, (z, yp(1), x, c), sent, first)
-                send(at, at, (z, yp(-1), x, c), sent, second)
+                at = block(buf, zp(-d), y)
+                for direction, sem in zip((1, -1), near_in[key]):
+                    send(at, at, (z, yp(direction), x, c), sent, sem)
 
         def relay(key, ds):
-            for direction, h, sem in ((1, 0, y_sems[m][3][key][0]), (-1, 1, y_sems[m][3][key][1])):
-                wait(buf.at[pl.ds(0, len(ds)), 0], sem)
+            for direction, h in ((1, 0), (-1, 1)):
+                wait(blocks(buf, len(ds)), near_in[key][h])
                 for d in ds:
                     at = half(zp(-d), yp(-direction), h)
-                    send(at, at, (z, yp(direction), x, c), passed, y_sems[m][2])
+                    send(at, at, (z, yp(direction), x, c), passed, far_in)
 
         def pass_far(key, ds):
             pass_on(key, ds)
             for d in ds:
-                at = buf.at[zp(-d), y]
-                send(at, at, (z, yp(2), x, c), passed, y_sems[m][2])
+                at = block(buf, zp(-d), y)
+                send(at, at, (z, yp(2), x, c), passed, far_in)
 
         def near_done(key, ds):
-            for sem in y_sems[m][3][key]:
-                wait(buf.at[pl.ds(0, len(ds)), 0], sem)
+            for sem in near_in[key]:
+                wait(blocks(buf, len(ds)), sem)
 
         def done():
-            wait(buf.at[:, 0], y_sems[m][2])
+            wait(far_bytes, far_in)
 
         return pass_on, relay, pass_far, near_done, done
 
     mine = lax.rem(z, 2)
 
     def spread(m, buf):
-        pair = buf.shape[2] == 2
-        quarter = pl.ds(0, Z // 2)
-        whole = buf.at[:, 0, 0] if pair else buf.at[quarter, 0, 0]
-        part_half = buf.at[quarter, 0, 0] if pair else buf.at[pl.ds(0, Z // 4), 0, 0]
-        all3 = buf.at[:, pl.ds(0, 3), 0] if pair else buf.at[quarter, pl.ds(0, 3), 0]
-        sent = send_group(buf.at[:, 0] if pair else buf.at[:, 0, 0])
+        pair = buf.shape[0] == Z
+        whole = buf.at[:, 0, 0]
+        part_half = buf.at[pl.ds(0, buf.shape[0] // 2), 0, 0]
+        all3 = buf.at[:, pl.ds(0, 3), 0] if pair else buf.at[:, 0, pl.ds(0, 3)]
+        swapped, swap_in = send_group(all3), new_sem()
+        ways = ((1, 0), (-1, 1))
+
+        def piece(row, part, half=None):
+            n = buf.shape[0] if half is None else buf.shape[0] // 2
+            zs = pl.ds((half or 0) * n, n)
+            return buf.at[zs, row, part] if pair else buf.at[zs, part, row]
+
+        def swap_rows():
+            for direction, h in ways:
+                at = piece(yp(-direction), mine)
+                send(at, at, (zp(direction), y, x, c), swapped, swap_in)
+
+        def swap_far():
+            for direction, h in ways:
+                at = piece(yp(2), mine, h)
+                send(at, at, (zp(direction), y, x, c), swapped, swap_in)
+
+        def done():
+            wait(all3, swap_in)
+
+        if m == "ou0":
+            return swap_rows, swap_far, done
+        sent = send_group(buf.at[:, 0] if pair else buf.at[:, :, 0])
         passed = send_group(whole)
-        swapped = send_group(all3)
-        row_in, far_in, swap_in = [new_sem(), new_sem()], [new_sem(), new_sem()], new_sem()
-        ways = ((1, 0), (-1, 1))
-
-        def piece(row, part, half=None):
-            if pair:
-                n = Z if half is None else Z // 2
-                return buf.at[pl.ds((half or 0) * Z // 2, n), row, part]
-            n = Z // 2 if half is None else Z // 4
-            return buf.at[pl.ds(part * (Z // 2) + (half or 0) * Z // 4, n), row, 0]
+        row_in, far_in = [new_sem(), new_sem()], [new_sem(), new_sem()]
 
         def a():
             for direction, h in ways:
@@ -194,18 +212,12 @@
                 wait(whole, row_in[h])
                 at = piece(yp(-direction), mine, h)
                 send(at, at, (z, yp(direction), x, c), passed, far_in[h])
-            for direction, h in ways:
-                at = piece(yp(-direction), mine)
-                send(at, at, (zp(direction), y, x, c), swapped, swap_in)
+            swap_rows()
 
         def e():
-            for direction, h in ways:
+            for _, h in ways:
                 wait(part_half, far_in[h])
-                at = piece(yp(2), mine, h)
-                send(at, at, (zp(direction), y, x, c), swapped, swap_in)
-
-        def done():
-            wait(all3, swap_in)
+            swap_far()
 
         return a, b, e, done
 
@@ -215,11 +227,11 @@
         near_in, far_in, mate = new_sem(), new_sem(), new_sem()
 
         def slot(d):
-            return buf.at[xp(d) * C + c, h]
+            return buf.at[xp(d) * C + 1 - c, h]
 
         def begin():
             for d, sem in ((2, far_in), (1, near_in), (-1, near_in)):
-                send(me, me, (z, y, xp(d), c), out, sem)
+                send(me, me, (z, y, xp(d), 1 - c), out, sem)
             send(me, me, other, out, mate)
 
         def near():
@@ -323,7 +335,8 @@
             v = (f[k, h].astype(F32) - mean) * scale * cg[k, pl.ds(layer, 1), :]
             act = (v * sigmoid(v)).astype(BF16)
             for hi in range(2):
-                w = ou[hi * TP + k, :, 0].reshape(128, cols)
+                slot = lax.rem(tp + hi * TP + lax.rem(k - tp + 12, TP) + Z - 4, Z)
+                w = ou[lax.div(slot, 2), lax.rem(slot, 2)].reshape(128, cols)
                 total[hi] = total[hi] + lax.dot_general(
                     act, w, (((1,), (1,)), ((), ())), preferred_element_type=F32
                 )
@@ -339,13 +352,13 @@
     perm_recv = new_sem()
     perm = [
         pltpu.make_async_remote_copy(
-            src_ref=ow.at[layer], dst_ref=buf.at[zhi * TP + tp, y, 0], send_sem=perm_send, recv_sem=perm_recv,
-            device_id=partner, device_id_type=MESH,
+            src_ref=ow.at[layer], dst_ref=block(buf, to_z, y), send_sem=perm_send, recv_sem=perm_recv,
+            device_id=goes_to, device_id_type=MESH,
         )
         for layer, buf in ((0, ou0), (1, ou1))
     ]
     drains.pop()
-    stay = [pltpu.make_async_copy(ow.at[layer], buf.at[z, y, 0], perm_recv) for layer, buf in ((0, ou0), (1, ou1))]
+    stay = [pltpu.make_async_copy(ow.at[layer], block(buf, z, y), perm_recv) for layer, buf in ((0, ou0), (1, ou1))]
 
     def perm_start():
         @pl.when(far)
@@ -362,7 +375,8 @@
         wait(ow, perm_recv)
 
     pass_vg, relay_vg, far_vg, near_vg, done_vg = y_group("vg0", vg0)
-    ou0_a, ou0_b, ou0_c, ou0_done = spread("ou0", ou0)
+    pass_ou, relay_ou, far_ou, near_ou, done_ou = y_group("ou0", ou0)
+    ou0_swap_rows, ou0_swap_far, ou0_done = spread("ou0", ou0)
     vg1_a, vg1_b, vg1_c, vg1_done = spread("vg1", vg1)
     ou1_a, ou1_b, ou1_c, ou1_done = spread("ou1", ou1)
 
@@ -391,46 +405,64 @@
 
     ring = [[0]] + [brought(RING, s) for s in range(4)]
 
-    def ring_step(m, buf, s):
-        z_wait(m, buf, RING, s - 1)
-        if s < 4:
-            z_stage(m, buf, RING, s)
+    def go_on(m, buf, plan, s):
+        z_wait(m, buf, plan, s - 1)
+        if s < len(plan):
+            z_stage(m, buf, plan, s)
+
+    def vg1_step(s):
+        go_on("vg1", vg1, RING, s)
+
+    def ou0_step(s):
+        go_on("ou0", ou0, RING, s)
+
+    def ou1_step(s):
+        go_on("ou1", ou1, RING, s)
+
+    even = [[d for d in ds if d % 2 == 0] for ds in ring]
 
     with scope("stage1"):
         vg0_stage(1)
         pass_vg(1, ring[1])
         relay_vg(0, ring[0])
+        perm_done()
+        z_stage("ou0", ou0, RING, 0)
+        pass_ou(0, even[0])
     with scope("stage2"):
         vg0_stage(2)
         pass_vg(2, ring[2])
         relay_vg(1, ring[1])
-        perm_done()
-        z_stage("ou0", ou0, RING, 0)
-        ring_step("vg1", vg1, 1)
+        ou0_step(1)
+        pass_ou(1, even[1])
+        vg1_step(1)
     with scope("stage3"):
         vg0_stage(3)
         pass_vg(3, ring[3])
         relay_vg(2, ring[2])
-        ring_step("ou0", ou0, 1)
-        ring_step("vg1", vg1, 2)
+        ou0_step(2)
+        pass_ou(2, even[2])
+        relay_ou(0, even[0])
+        vg1_step(2)
     with scope("stage4"):
         vg0_stage(4)
         far_vg(4, ring[4])
         relay_vg(3, ring[3])
-        ring_step("ou0", ou0, 2)
-        ring_step("vg1", vg1, 3)
+        ou0_step(3)
+        pass_ou(3, even[3])
+        relay_ou(1, even[1])
+        vg1_step(3)
         z_stage("ou1", ou1, RING, 0)
-    with scope("stage5"):
-        ring_step("ou0", ou0, 3)
     with scope("vg0done"):
         near_vg(4, ring[4])
         done_vg()
 
-    def layer_head(layer, vg, gb, hbuf, f, ready):
+    def layer_head(layer, vg, gb, hbuf, f, ready, hook):
         first, second = gather_tp(f, 1), gather_tp(f, 0)
         with scope("proj"):
             project(layer, vg, gb, 1)
         arrives, sent = halo(gb, hbuf)
+        with scope("hookp"):
+            hook()
         with scope("projb"):
             ready()
             project(layer, vg, gb, 0)
@@ -454,11 +486,10 @@
             hooks[1]()
         with scope("ag1"):
             first[1]()
-            second[1]()
+            first[2]()
         with scope("hook1"):
             hooks[2]()
         with scope("ag1b"):
-            first[2]()
             first[3]()
         with scope("hook2"):
             hooks[3]()
@@ -467,8 +498,8 @@
             activate_and_project(layer, f, ou, nxt, 1)
         first2[0]()
         with scope("ag1c"):
-            second[2]()
-            second[3]()
+            for step in second[1:]:
+                step()
         with scope("actb"):
             activate_and_project(layer, f, ou, nxt, 0)
         second2[0]()
@@ -476,33 +507,38 @@
             hooks[4]()
         with scope("ag2"):
             first2[1]()
-            second2[1]()
+            first2[2]()
         with scope("hook4"):
             hooks[5]()
         with scope("ag2b"):
-            first2[2]()
             first2[3]()
         return second2
 
     def nothing():
         pass
 
-    first, second, arrives, sent0 = layer_head(0, vg0, gb0, h0, f0, nothing)
+    def hook0p():
+        ou0_step(4)
+        far_ou(4, even[4])
+        relay_ou(2, even[2])
+        relay_ou(3, even[3])
+        ou1_step(1)
+
+    first, second, arrives, sent0 = layer_head(0, vg0, gb0, h0, f0, nothing, hook0p)
 
     def hook00():
-        ring_step("ou0", ou0, 4)
-        ou0_a()
-        ring_step("vg1", vg1, 4)
+        vg1_step(4)
         vg1_a()
-        ring_step("ou1", ou1, 1)
 
     def hook00b():
-        ring_step("ou1", ou1, 2)
-        ou0_b()
+        near_ou(4, even[4])
+        ou0_swap_rows()
+        ou1_step(2)
 
     def hook01():
-        ou0_c()
-        ring_step("ou1", ou1, 3)
+        done_ou()
+        ou0_swap_far()
+        ou1_step(3)
 
     def hook02():
         vg1_b()
@@ -510,26 +546,31 @@
         ou0_done()
 
     def hook03():
-        ring_step("ou1", ou1, 4)
+        ou1_step(4)
+
+    def hook04():
         vg1_c()
         ou1_a()
 
-    rest = layer_tail(0, f0, ou0, s1, (first, second), arrives, (hook00, hook00b, hook01, hook02, hook03, nothing))
+    rest = layer_tail(
+        0, f0, ou0, s1, (first, second), arrives, (hook00, hook00b, hook01, hook02, hook03, hook04)
+    )
     with scope("norm1"):
         normalise(1, 1)
 
     def ready():
         with scope("ag2c"):
-            rest[2]()
-            rest[3]()
+            for step in rest[1:]:
+                step()
         normalise(1, 0)
 
     with scope("vg1done"):
+        ou1_b()
         vg1_done()
 
-    first, second, arrives, sent1 = layer_head(1, vg1, gb1, h1, f1, ready)
+    first, second, arrives, sent1 = layer_head(1, vg1, gb1, h1, f1, ready, nothing)
     rest1 = layer_tail(
-        1, f1, ou1, s2, (first, second), arrives, (nothing, ou1_b, ou1_c, ou1_done, nothing, nothing)
+        1, f1, ou1, s2, (first, second), arrives, (nothing, ou1_c, nothing, ou1_done, nothing, nothing)
     )
 
     def write(h):
@@ -538,8 +579,8 @@
 
     write(1)
     with scope("ag2c"):
-        rest1[2]()
-        rest1[3]()
+        for step in rest1[1:]:
+            step()
     write(0)
 
     with scope("out"):
@@ -563,14 +604,14 @@
     taps = jnp.swapaxes(conv_taps, 0, 1)
     return pl.pallas_call(
         kernel,
-        out_shape=jax.ShapeDtypeStruct((rows, width), BF16),
+        out_shape=pltpu.VMEM((rows, width), BF16),
         in_specs=[hbm, vmem, hbm, hbm, vmem, hbm, hbm],
         out_specs=vmem,
         scratch_shapes=[
             pltpu.VMEM((Z, Y, 2, depth, cols), BF16),
             pltpu.VMEM((Z, Y, 2, depth, cols), BF16),
-            pltpu.VMEM((Z, Y, 1, depth, cols), BF16),
-            pltpu.VMEM((Z, Y, 1, depth, cols), BF16),
+            pltpu.VMEM((Z // 2, 2, Y, depth, cols), BF16),
+            pltpu.VMEM((Z // 2, 2, Y, depth, cols), BF16),
             pltpu.VMEM((rows, width), BF16),
             pltpu.VMEM((TP, 2, 2, rows // 2, 128), BF16),
             pltpu.VMEM((TP, 2, 2, rows // 2, 128), BF16),

time: 98.3 us -> 87.5 us (0.89)
  Pallas kernels: 95.7 us -> 86.3 us
  local copies, waits for them, and re-layouts: 2.3 us -> 0.97 us
    pallas_call x1, Pallas kernels: 95.7 us -> 86.3 us  [body(): pl.pallas_call(kernel, out_shape=pltpu.VMEM((rows, width), BF16), in_spec...]
    unnamed x1, local copies, waits for them, and re-layouts: 2.3 us -> 0.97 us
where the time goes in v3:
time: 87.5 us; the launch traced here: 87.3 us
  Pallas kernels  86.3 us (99%)
  local copies, waits for them, and re-layouts  0.97 us (1%)
    pallas_call x1, Pallas kernels, body(): pl.pallas_call(kernel, out_shape=pltpu.VMEM((rows, width), BF16), in_spec...  86.3 us

profile of v3, /device:TPU:1, one launch (start us, length us, event | category | flops | bytes accessed | tf_op | source)
XLA Modules:
  0.0 87.3 jit_solution(9821401392917917017)
XLA Ops:
  0.0 86.3 %shard_map.73 = bf16[256,2048]{1,0:T(8,128)(2,1)S(1)} custom-call(bf16[256,2048]{1,0:T(8,128)(2,1)} %stream_hbm.1, f32[2,2048]{1,0:T(2,128)} %ngain.1, bf16[2,32,256]{2,1,0:T(8,128)(2,1)} %vw.1, bf16[2,32,256]{2,1,0:T(8,128)(2,1)} %gw.1, f32[31,2,256]{2,1,0:T(2,128)} %bitcast.2, f32[2,256]{1,0:T(2,128)} %cgain.1, bf16[2,32,256]{2,1,0:T(8,128)(2,1)} %bitcast.3), custom_call_target="tpu_custom_call" | custom-call | tf_op jit(solution)/shard_map/pallas_call | solution.py:605
  86.3 1.0 %copy.9 = bf16[256,2048]{1,0:T(8,128)(2,1)} copy(bf16[256,2048]{1,0:T(8,128)(2,1)S(1)} %shard_map.73) | data formatting | bytes 2097152

commit v4 on v3

--- a/solution.py
+++ b/solution.py
@@ -12,7 +12,7 @@
 EPS = 1e-05
 F32 = jnp.float32
 BF16 = jnp.bfloat16
-N_SEMS = 113
+N_SEMS = 143
 HALO = 32
 RING = [
     [(2 * s, tuple(d for d in (2 * s + 2, 2 * s + 1) if d <= Z // 2)),
@@ -20,6 +20,7 @@
     for s in range(4)
 ]
 VMEM_LIMIT = 60_000_000
+CHUNKS = 4
 scope = jax.named_scope
 
 
@@ -28,8 +29,8 @@
 
 
 def kernel(
-    stream_hbm, ngain, vw, gw, taps, cgain, ow, out_ref,
-    vg0, vg1, ou0, ou1, xs, s1, s2, f0, f1, nb, gx, h0, h1, gb0, gb1, cg, sems,
+    stream_hbm, ngain_hbm, vw, gw, taps_hbm, cgain, ow, out_ref,
+    taps, ngain, vg0, vg1, ou0, ou1, xs, s1, s2, f0, f1, nb, gx, h0, h1, gb0, gb1, cg, sems,
 ):
     z, y, x, c = (lax.axis_index(a) for a in ("z", "y", "x", "c"))
     tp = x * C + c
@@ -65,7 +66,7 @@
     def xp(d):
         return lax.rem(x + d + X, X)
 
-    own_sem = [new_sem() for _ in range(4)]
+    own_sem = [new_sem() for _ in range(6)]
     own = [
         pltpu.make_async_copy(vw.at[0], vg0.at[z, y, 0], own_sem[0]),
         pltpu.make_async_copy(gw.at[0], vg0.at[z, y, 1], own_sem[0]),
@@ -73,6 +74,8 @@
         pltpu.make_async_copy(gw.at[1], vg1.at[z, y, 1], own_sem[1]),
         pltpu.make_async_copy(stream_hbm, xs, own_sem[2]),
         pltpu.make_async_copy(cgain, cg.at[tp], own_sem[3]),
+        pltpu.make_async_copy(ngain_hbm, ngain, own_sem[4]),
+        pltpu.make_async_copy(taps_hbm, taps, own_sem[5]),
     ]
     for copy in own:
         copy.start()
@@ -171,17 +174,19 @@
 
     mine = lax.rem(z, 2)
 
-    def spread(m, buf):
+    def spread(m, buf, first=0, count=None):
         pair = buf.shape[0] == Z
-        whole = buf.at[:, 0, 0]
-        part_half = buf.at[pl.ds(0, buf.shape[0] // 2), 0, 0]
-        all3 = buf.at[:, pl.ds(0, 3), 0] if pair else buf.at[:, 0, pl.ds(0, 3)]
+        count = count or buf.shape[0]
+        some = pl.ds(first, count)
+        whole = buf.at[some, 0, 0]
+        part_half = buf.at[pl.ds(first, count // 2), 0, 0]
+        all3 = buf.at[some, pl.ds(0, 3), 0] if pair else buf.at[some, 0, pl.ds(0, 3)]
         swapped, swap_in = send_group(all3), new_sem()
         ways = ((1, 0), (-1, 1))
 
         def piece(row, part, half=None):
-            n = buf.shape[0] if half is None else buf.shape[0] // 2
-            zs = pl.ds((half or 0) * n, n)
+            n = count if half is None else count // 2
+            zs = pl.ds(first + (half or 0) * n, n)
             return buf.at[zs, row, part] if pair else buf.at[zs, part, row]
 
         def swap_rows():
@@ -199,7 +204,7 @@
 
         if m == "ou0":
             return swap_rows, swap_far, done
-        sent = send_group(buf.at[:, 0] if pair else buf.at[:, :, 0])
+        sent = send_group(buf.at[some, 0] if pair else buf.at[some, :, 0])
         passed = send_group(whole)
         row_in, far_in = [new_sem(), new_sem()], [new_sem(), new_sem()]
 
@@ -221,9 +226,12 @@
 
         return a, b, e, done
 
-    def gather_tp(buf, h):
+    def gather_tp(buf):
+        out = send_group(buf.at[pl.ds(0, TP - 1)])
+        return [gather_chunk(buf, h, out) for h in range(CHUNKS)]
+
+    def gather_chunk(buf, h, out):
         me, other = buf.at[tp, h], (z, y, x, 1 - c)
-        out = send_group(buf.at[pl.ds(0, TP - 1), h])
         near_in, far_in, mate = new_sem(), new_sem(), new_sem()
 
         def slot(d):
@@ -239,58 +247,56 @@
             for d in (1, -1):
                 send(slot(d), slot(d), other, out, mate)
 
-        def last():
+        def far_one():
             wait(me, far_in)
             send(slot(2), slot(2), other, out, mate)
 
         def done():
             wait(buf.at[pl.ds(0, X), h], mate)
 
-        return begin, near, last, done
+        return begin, near, far_one, done
 
     rows_all, width = xs.shape
     cols = gx.shape[2] * 2
-    nh = rows_all // 2
+    nh = rows_all // CHUNKS
+    last = CHUNKS - 1
 
     def normalise(layer, h):
-        n = 64
-        for i in range(nh // n):
-            rows = pl.ds(h * nh + i * n, n)
-
-            def group(g):
-                if layer == 0:
-                    return xs[rows, pl.ds(g * 128, 128)].astype(F32)
-                return s1[g % TP, h, g // TP, pl.ds(i * n, n), :].astype(F32)
-
-            total = None
-            for g in range(width // 128):
-                wide = group(g)
-                total = wide * wide if total is None else total + wide * wide
-            scale = lax.rsqrt(jnp.sum(total, axis=1, keepdims=True) / width + EPS)
-            for g in range(width // 128):
-                gain = ngain[pl.ds(layer, 1), pl.ds(g * 128, 128)]
-                nb[rows, pl.ds(g * 128, 128)] = (group(g) * scale * gain).astype(BF16)
+        rows = pl.ds(h * nh, nh)
+
+        def group(g):
+            if layer == 0:
+                return xs[rows, pl.ds(g * 128, 128)].astype(F32)
+            return s1[g % TP, h, g // TP].astype(F32)
+
+        total = None
+        for g in range(width // 128):
+            wide = group(g)
+            total = wide * wide if total is None else total + wide * wide
+        scale = lax.rsqrt(jnp.sum(total, axis=1, keepdims=True) / width + EPS)
+        for g in range(width // 128):
+            gain = ngain[pl.ds(layer, 1), pl.ds(g * 128, 128)]
+            nb[rows, pl.ds(g * 128, 128)] = (group(g) * scale * gain).astype(BF16)
 
     def project(layer, buf, gb, h):
         n = nb[pl.ds(h * nh, nh), :]
         value = jnp.dot(n, buf[:, :, 0].reshape(width, cols), preferred_element_type=F32)
         gate = jnp.dot(n, buf[:, :, 1].reshape(width, cols), preferred_element_type=F32)
         gated = (value * sigmoid(gate)).astype(BF16)
-        if h:
+        if h == last:
             gb[...] = gated[nh - HALO :]
         wide = gated.astype(F32)
         for j in range(2):
             gx[j, HALO + h * nh : HALO + h * nh + nh, :] = wide[:, j * 128 : (j + 1) * 128]
 
-    def convolve(layer, f, block):
-        n = 64
-        first = block * n + HALO - 30
+    def convolve(layer, f, h):
+        first = h * nh + HALO - 30
         for j in range(2):
             acc = None
             for k in range(31):
-                term = taps[k, pl.ds(layer, 1), pl.ds(j * 128, 128)] * gx[j, first + k : first + k + n, :]
+                term = taps[k, pl.ds(layer, 1), pl.ds(j * 128, 128)] * gx[j, first + k : first + k + nh, :]
                 acc = term if acc is None else acc + term
-            f[tp, block // 2, (block % 2) * n : (block % 2) * n + n, j * 128 : (j + 1) * 128] = acc.astype(BF16)
+            f[tp, h, :, j * 128 : (j + 1) * 128] = acc.astype(BF16)
 
     def halo(gb, hbuf):
         copy = pltpu.make_async_remote_copy(
@@ -377,7 +383,7 @@
     pass_vg, relay_vg, far_vg, near_vg, done_vg = y_group("vg0", vg0)
     pass_ou, relay_ou, far_ou, near_ou, done_ou = y_group("ou0", ou0)
     ou0_swap_rows, ou0_swap_far, ou0_done = spread("ou0", ou0)
-    vg1_a, vg1_b, vg1_c, vg1_done = spread("vg1", vg1)
+    vg1_a, vg1_b, vg1_c, vg1_done = zip(*(spread("vg1", vg1, n, Z // 2) for n in (0, Z // 2)))
     ou1_a, ou1_b, ou1_c, ou1_done = spread("ou1", ou1)
 
     def vg0_stage(s):
@@ -399,8 +405,9 @@
         to = lax.rem(tp + d, TP)
         send(cg.at[tp], cg.at[tp], (z, y, lax.div(to, C), lax.rem(to, C)), gain_sent, gain_in)
     wait(xs, own_sem[2])
+    wait(ngain, own_sem[4])
     with scope("norm0"):
-        for h in range(2):
+        for h in range(CHUNKS):
             normalise(0, h)
 
     ring = [[0]] + [brought(RING, s) for s in range(4)]
@@ -452,70 +459,64 @@
         relay_ou(1, even[1])
         vg1_step(3)
         z_stage("ou1", ou1, RING, 0)
+    wait(taps, own_sem[5])
     with scope("vg0done"):
         near_vg(4, ring[4])
         done_vg()
 
-    def layer_head(layer, vg, gb, hbuf, f, ready, hook):
-        first, second = gather_tp(f, 1), gather_tp(f, 0)
-        with scope("proj"):
-            project(layer, vg, gb, 1)
-        arrives, sent = halo(gb, hbuf)
-        with scope("hookp"):
-            hook()
-        with scope("projb"):
-            ready()
-            project(layer, vg, gb, 0)
-        with scope("conv"):
-            convolve(layer, f, 2)
-            convolve(layer, f, 3)
-        first[0]()
-        with scope("convb"):
-            convolve(layer, f, 1)
-        return first, second, arrives, sent
-
-    def layer_tail(layer, f, ou, nxt, parts, arrives, hooks):
-        first, second = parts
-        with scope("hook0"):
-            hooks[0]()
+    order = range(CHUNKS - 1, -1, -1)
+
+    def receive(gather, h, between=None):
+        if h == last:
+            gather[h][1]()
+            gather[h][2]()
+            if between:
+                between()
+        if h:
+            gather[h - 1][1]()
+            gather[h - 1][2]()
+        gather[h][3]()
+
+    def layer_of(layer, vg, gb, hbuf, f, ou, nxt, source, weights_ready, hooks):
+        first, second = gather_tp(f), gather_tp(nxt)
+
+        def hook(name):
+            if name in hooks:
+                with scope(name):
+                    hooks[name]()
+
+        for h in order:
+            if source is not None:
+                with scope("get%d" % h):
+                    receive(source, h)
+                normalise(layer, h)
+            if h == last:
+                weights_ready()
+            with scope("proj%d" % h):
+                project(layer, vg, gb, h)
+            if h == last:
+                arrives, sent = halo(gb, hbuf)
+                hook("hookp")
+            else:
+                convolve(layer, f, h + 1)
+                first[h + 1][0]()
+                hook("head%d" % h)
+        hook("hook0")
         with scope("halo"):
             arrives()
             convolve(layer, f, 0)
-        second[0]()
-        with scope("hook0b"):
-            hooks[1]()
-        with scope("ag1"):
-            first[1]()
-            first[2]()
-        with scope("hook1"):
-            hooks[2]()
-        with scope("ag1b"):
-            first[3]()
-        with scope("hook2"):
-            hooks[3]()
-        first2, second2 = gather_tp(nxt, 1), gather_tp(nxt, 0)
-        with scope("act"):
-            activate_and_project(layer, f, ou, nxt, 1)
-        first2[0]()
-        with scope("ag1c"):
-            for step in second[1:]:
-                step()
-        with scope("actb"):
-            activate_and_project(layer, f, ou, nxt, 0)
-        second2[0]()
-        with scope("hook3"):
-            hooks[4]()
-        with scope("ag2"):
-            first2[1]()
-            first2[2]()
-        with scope("hook4"):
-            hooks[5]()
-        with scope("ag2b"):
-            first2[3]()
-        return second2
-
-    def nothing():
-        pass
+        first[0][0]()
+        hook("hook0b")
+        for h in order:
+            with scope("ag%d" % h):
+                receive(first, h, lambda: hook("hook1"))
+            if h == last:
+                hook("hook2")
+            with scope("act%d" % h):
+                activate_and_project(layer, f, ou, nxt, h)
+            second[h][0]()
+            hook("after%d" % h)
+        return second, sent
 
     def hook0p():
         ou0_step(4)
@@ -524,64 +525,50 @@
         relay_ou(3, even[3])
         ou1_step(1)
 
-    first, second, arrives, sent0 = layer_head(0, vg0, gb0, h0, f0, nothing, hook0p)
-
     def hook00():
         vg1_step(4)
-        vg1_a()
+        vg1_a[0]()
 
     def hook00b():
         near_ou(4, even[4])
         ou0_swap_rows()
+        vg1_a[1]()
         ou1_step(2)
 
     def hook01():
         done_ou()
         ou0_swap_far()
+        vg1_b[0]()
         ou1_step(3)
 
     def hook02():
-        vg1_b()
+        vg1_b[1]()
         wait(cg.at[pl.ds(0, TP - 1)], gain_in)
         ou0_done()
 
     def hook03():
         ou1_step(4)
-
-    def hook04():
-        vg1_c()
         ou1_a()
 
-    rest = layer_tail(
-        0, f0, ou0, s1, (first, second), arrives, (hook00, hook00b, hook01, hook02, hook03, hook04)
-    )
-    with scope("norm1"):
-        normalise(1, 1)
+    hooks0 = {
+        "hookp": hook0p, "hook0": hook00, "hook0b": hook00b, "hook1": hook01, "hook2": hook02,
+        "after3": vg1_c[0], "after2": vg1_c[1], "after1": hook03,
+    }
+    rest, sent0 = layer_of(0, vg0, gb0, h0, f0, ou0, s1, None, lambda: None, hooks0)
 
     def ready():
-        with scope("ag2c"):
-            for step in rest[1:]:
-                step()
-        normalise(1, 0)
-
-    with scope("vg1done"):
-        ou1_b()
-        vg1_done()
-
-    first, second, arrives, sent1 = layer_head(1, vg1, gb1, h1, f1, ready, nothing)
-    rest1 = layer_tail(
-        1, f1, ou1, s2, (first, second), arrives, (nothing, ou1_c, nothing, ou1_done, nothing, nothing)
-    )
-
-    def write(h):
+        with scope("vg1done"):
+            ou1_b()
+            vg1_done[0]()
+            vg1_done[1]()
+
+    hooks1 = {"head1": ou1_c, "hook2": ou1_done}
+    rest1, sent1 = layer_of(1, vg1, gb1, h1, f1, ou1, s2, rest, ready, hooks1)
+    for h in order:
+        with scope("last%d" % h):
+            receive(rest1, h)
         for g in range(width // 128):
             out_ref[h * nh : (h + 1) * nh, g * 128 : (g + 1) * 128] = s2[g % TP, h, g // TP]
-
-    write(1)
-    with scope("ag2c"):
-        for step in rest1[1:]:
-            step()
-    write(0)
 
     with scope("out"):
         for ref, sem in drains:
@@ -605,18 +592,20 @@
     return pl.pallas_call(
         kernel,
         out_shape=pltpu.VMEM((rows, width), BF16),
-        in_specs=[hbm, vmem, hbm, hbm, vmem, hbm, hbm],
+        in_specs=[hbm] * 7,
         out_specs=vmem,
         scratch_shapes=[
+            pltpu.VMEM(taps.shape, F32),
+            pltpu.VMEM(norm_gain.shape, F32),
             pltpu.VMEM((Z, Y, 2, depth, cols), BF16),
             pltpu.VMEM((Z, Y, 2, depth, cols), BF16),
             pltpu.VMEM((Z // 2, 2, Y, depth, cols), BF16),
             pltpu.VMEM((Z // 2, 2, Y, depth, cols), BF16),
             pltpu.VMEM((rows, width), BF16),
-            pltpu.VMEM((TP, 2, 2, rows // 2, 128), BF16),
-            pltpu.VMEM((TP, 2, 2, rows // 2, 128), BF16),
-            pltpu.VMEM((TP, 2, rows // 2, cols), BF16),
-            pltpu.VMEM((TP, 2, rows // 2, cols), BF16),
+            pltpu.VMEM((TP, CHUNKS, 2, rows // CHUNKS, 128), BF16),
+            pltpu.VMEM((TP, CHUNKS, 2, rows // CHUNKS, 128), BF16),
+            pltpu.VMEM((TP, CHUNKS, rows // CHUNKS, cols), BF16),
+            pltpu.VMEM((TP, CHUNKS, rows // CHUNKS, cols), BF16),
             pltpu.VMEM((rows, width), BF16),
             pltpu.VMEM((2, rows + HALO, 128), F32),
             pltpu.VMEM((HALO, cols), BF16),

time: 87.5 us -> 83.2 us (0.951)
  Pallas kernels: 86.3 us -> 82.1 us
    pallas_call x1, Pallas kernels: 86.3 us -> 82.1 us  [body(): pl.pallas_call(kernel, out_shape=pltpu.VMEM((rows, width), BF16), in_spec...]
where the time goes in v4:
time: 83.2 us; the launch traced here: 83.1 us
  Pallas kernels  82.1 us (99%)
  local copies, waits for them, and re-layouts  0.97 us (1%)
    pallas_call x1, Pallas kernels, body(): pl.pallas_call(kernel, out_shape=pltpu.VMEM((rows, width), BF16), in_spec...  82.1 us

profile of v4, /device:TPU:1, one launch (start us, length us, event | category | flops | bytes accessed | tf_op | source)
XLA Modules:
  0.0 83.1 jit_solution(2784684917881789749)
XLA Ops:
  0.0 82.1 %shard_map.73 = bf16[256,2048]{1,0:T(8,128)(2,1)S(1)} custom-call(bf16[256,2048]{1,0:T(8,128)(2,1)} %stream_hbm.1, f32[2,2048]{1,0:T(2,128)} %ngain_hbm.1, bf16[2,32,256]{2,1,0:T(8,128)(2,1)} %vw.1, bf16[2,32,256]{2,1,0:T(8,128)(2,1)} %gw.1, f32[31,2,256]{2,1,0:T(2,128)} %bitcast.2, f32[2,256]{1,0:T(2,128)} %cgain.1, bf16[2,32,256]{2,1,0:T(8,128)(2,1)} %bitcast.3), custom_call_target="tpu_custom_call" | custom-call | tf_op jit(solution)/shard_map/pallas_call | solution.py:592
  82.1 1.0 %copy.9 = bf16[256,2048]{1,0:T(8,128)(2,1)} copy(bf16[256,2048]{1,0:T(8,128)(2,1)S(1)} %shard_map.73) | data formatting | bytes 2097152

commit v5 on v4

--- a/solution.py
+++ b/solution.py
@@ -12,7 +12,7 @@
 EPS = 1e-05
 F32 = jnp.float32
 BF16 = jnp.bfloat16
-N_SEMS = 143
+N_SEMS = 106
 HALO = 32
 RING = [
     [(2 * s, tuple(d for d in (2 * s + 2, 2 * s + 1) if d <= Z // 2)),
@@ -226,35 +226,34 @@
 
         return a, b, e, done
 
-    def gather_tp(buf):
+    tp_sems = {}
+
+    def gather_tp(buf, kind):
+        if kind not in tp_sems:
+            tp_sems[kind] = [(new_sem(), new_sem()) for _ in range(CHUNKS)]
         out = send_group(buf.at[pl.ds(0, TP - 1)])
-        return [gather_chunk(buf, h, out) for h in range(CHUNKS)]
-
-    def gather_chunk(buf, h, out):
+        return [gather_chunk(buf, h, out, *tp_sems[kind][h]) for h in range(CHUNKS)]
+
+    def gather_chunk(buf, h, out, chips, mate):
         me, other = buf.at[tp, h], (z, y, x, 1 - c)
-        near_in, far_in, mate = new_sem(), new_sem(), new_sem()
 
         def slot(d):
             return buf.at[xp(d) * C + 1 - c, h]
 
         def begin():
-            for d, sem in ((2, far_in), (1, near_in), (-1, near_in)):
-                send(me, me, (z, y, xp(d), 1 - c), out, sem)
+            for d in (2, 1, -1):
+                send(me, me, (z, y, xp(d), 1 - c), out, chips)
             send(me, me, other, out, mate)
 
-        def near():
-            wait(buf.at[pl.ds(0, 2), h], near_in)
-            for d in (1, -1):
+        def forward():
+            wait(buf.at[pl.ds(0, X - 1), h], chips)
+            for d in (1, -1, 2):
                 send(slot(d), slot(d), other, out, mate)
-
-        def far_one():
-            wait(me, far_in)
-            send(slot(2), slot(2), other, out, mate)
 
         def done():
             wait(buf.at[pl.ds(0, X), h], mate)
 
-        return begin, near, far_one, done
+        return begin, forward, done
 
     rows_all, width = xs.shape
     cols = gx.shape[2] * 2
@@ -387,11 +386,10 @@
     ou1_a, ou1_b, ou1_c, ou1_done = spread("ou1", ou1)
 
     def vg0_stage(s):
-        for part in range(2):
-            if s:
-                z_wait("vg0", vg0, RING, s - 1, part)
-            if s < 4:
-                z_stage("vg0", vg0, RING, s, part)
+        if s:
+            z_wait("vg0", vg0, RING, s - 1)
+        if s < 4:
+            z_stage("vg0", vg0, RING, s)
 
     wait(vg0.at[z, y], own_sem[0])
     vg0_stage(0)
@@ -469,16 +467,14 @@
     def receive(gather, h, between=None):
         if h == last:
             gather[h][1]()
-            gather[h][2]()
             if between:
                 between()
         if h:
             gather[h - 1][1]()
-            gather[h - 1][2]()
-        gather[h][3]()
+        gather[h][2]()
 
     def layer_of(layer, vg, gb, hbuf, f, ou, nxt, source, weights_ready, hooks):
-        first, second = gather_tp(f), gather_tp(nxt)
+        first, second = gather_tp(f, 1), gather_tp(nxt, 2)
 
         def hook(name):
             if name in hooks:

time: 83.2 us -> 82.6 us (level)
  no operation moved by 1% of the time
where the time goes in v5:
time: 82.6 us; the launch traced here: 82.5 us
  Pallas kernels  81.5 us (99%)
  local copies, waits for them, and re-layouts  0.97 us (1%)
    pallas_call x1, Pallas kernels, body(): pl.pallas_call(kernel, out_shape=pltpu.VMEM((rows, width), BF16), in_spec...  81.5 us

profile of v5, /device:TPU:1, one launch (start us, length us, event | category | flops | bytes accessed | tf_op | source)
XLA Modules:
  0.0 82.5 jit_solution(11784350222939324324)
XLA Ops:
  0.0 81.5 %shard_map.73 = bf16[256,2048]{1,0:T(8,128)(2,1)S(1)} custom-call(bf16[256,2048]{1,0:T(8,128)(2,1)} %stream_hbm.1, f32[2,2048]{1,0:T(2,128)} %ngain_hbm.1, bf16[2,32,256]{2,1,0:T(8,128)(2,1)} %vw.1, bf16[2,32,256]{2,1,0:T(8,128)(2,1)} %gw.1, f32[31,2,256]{2,1,0:T(2,128)} %bitcast.2, f32[2,256]{1,0:T(2,128)} %cgain.1, bf16[2,32,256]{2,1,0:T(8,128)(2,1)} %bitcast.3), custom_call_target="tpu_custom_call" | custom-call | tf_op jit(solution)/shard_map/pallas_call | solution.py:588
  81.5 1.0 %copy.9 = bf16[256,2048]{1,0:T(8,128)(2,1)} copy(bf16[256,2048]{1,0:T(8,128)(2,1)S(1)} %shard_map.73) | data formatting | bytes 2097152

commit v6 on v5

--- a/solution.py
+++ b/solution.py
@@ -448,6 +448,7 @@
         pass_ou(2, even[2])
         relay_ou(0, even[0])
         vg1_step(2)
+        z_stage("ou1", ou1, RING, 0)
     with scope("stage4"):
         vg0_stage(4)
         far_vg(4, ring[4])
@@ -456,7 +457,7 @@
         pass_ou(3, even[3])
         relay_ou(1, even[1])
         vg1_step(3)
-        z_stage("ou1", ou1, RING, 0)
+        ou1_step(1)
     wait(taps, own_sem[5])
     with scope("vg0done"):
         near_vg(4, ring[4])
@@ -519,23 +520,24 @@
         far_ou(4, even[4])
         relay_ou(2, even[2])
         relay_ou(3, even[3])
-        ou1_step(1)
-
-    def hook00():
+        ou1_step(2)
+
+    def head02():
         vg1_step(4)
         vg1_a[0]()
+
+    def hook00():
+        vg1_a[1]()
 
     def hook00b():
         near_ou(4, even[4])
         ou0_swap_rows()
-        vg1_a[1]()
-        ou1_step(2)
-
-    def hook01():
+        ou1_step(3)
         done_ou()
         ou0_swap_far()
+
+    def hook01():
         vg1_b[0]()
-        ou1_step(3)
 
     def hook02():
         vg1_b[1]()
@@ -547,7 +549,7 @@
         ou1_a()
 
     hooks0 = {
-        "hookp": hook0p, "hook0": hook00, "hook0b": hook00b, "hook1": hook01, "hook2": hook02,
+        "hookp": hook0p, "head2": head02, "hook0": hook00, "hook0b": hook00b, "hook1": hook01, "hook2": hook02,
         "after3": vg1_c[0], "after2": vg1_c[1], "after1": hook03,
     }
     rest, sent0 = layer_of(0, vg0, gb0, h0, f0, ou0, s1, None, lambda: None, hooks0)

time: 82.6 us -> 81.8 us (level)
  no operation moved by 1% of the time
where the time goes in v6:
time: 81.8 us; the launch traced here: 81.7 us
  Pallas kernels  80.7 us (99%)
  local copies, waits for them, and re-layouts  0.97 us (1%)
    pallas_call x1, Pallas kernels, body(): pl.pallas_call(kernel, out_shape=pltpu.VMEM((rows, width), BF16), in_spec...  80.7 us

profile of v6, /device:TPU:1, one launch (start us, length us, event | category | flops | bytes accessed | tf_op | source)
XLA Modules:
  0.0 81.7 jit_solution(1785919089608767479)
XLA Ops:
  0.0 80.7 %shard_map.73 = bf16[256,2048]{1,0:T(8,128)(2,1)S(1)} custom-call(bf16[256,2048]{1,0:T(8,128)(2,1)} %stream_hbm.1, f32[2,2048]{1,0:T(2,128)} %ngain_hbm.1, bf16[2,32,256]{2,1,0:T(8,128)(2,1)} %vw.1, bf16[2,32,256]{2,1,0:T(8,128)(2,1)} %gw.1, f32[31,2,256]{2,1,0:T(2,128)} %bitcast.2, f32[2,256]{1,0:T(2,128)} %cgain.1, bf16[2,32,256]{2,1,0:T(8,128)(2,1)} %bitcast.3), custom_call_target="tpu_custom_call" | custom-call | tf_op jit(solution)/shard_map/pallas_call | solution.py:590
  80.7 1.0 %copy.9 = bf16[256,2048]{1,0:T(8,128)(2,1)} copy(bf16[256,2048]{1,0:T(8,128)(2,1)S(1)} %shard_map.73) | data formatting | bytes 2097152
